TPU v7x, 256 devices: a whole 4x4x8 slice. The times are simulated.
256 devices in a mesh: sp: 16 (over y, x), tp: 16 (over z, core).
Axes of the slice: x: 4, y: 4, z: 8, core: 2. Of those that a mesh axis runs over, the one named last changes fastest.
Arguments:
- residual: bfloat16 [16384, 2048], P(('sp', 'tp')), may hold values from -6 to 6
- wide_query: bfloat16 [16384, 1024], P('sp', 'tp'), may hold values from -8 to 8
- narrow_query: bfloat16 [16384, 1024], P('sp', 'tp'), may hold values from -8 to 8
- wide_keys: bfloat16 [16384, 256], P('sp'), may hold values from -6 to 6
- narrow_keys: bfloat16 [16384, 256], P('sp'), may hold values from -6 to 6
- wide_values: bfloat16 [16384, 256], P('sp'), may hold values from -6 to 6
- narrow_values: bfloat16 [16384, 256], P('sp'), may hold values from -6 to 6
- wide_query_gain: float32 [64], replicated, may hold values from 1.2 to 10
- wide_key_gain: float32 [64], replicated, may hold values from 1.2 to 10
- narrow_query_gain: float32 [32], replicated, may hold values from 1.2 to 10
- narrow_key_gain: float32 [32], replicated, may hold values from 1.2 to 10
- wide_out: bfloat16 [1024, 2048], P('tp'), may hold values from -0.25 to 0.25
- narrow_out: bfloat16 [1024, 2048], P('tp'), may hold values from -0.25 to 0.25
- first_gain: float32 [2048], replicated, may hold values from 0.1 to 1.9
- first_bias: float32 [2048], replicated, may hold values from -1.8 to 1.8
- route_ids: int32 [16384, 2], P(('sp', 'tp')), may hold values from 0 to 31, all different within a row; in each aligned block of 64 rows (0 to 63, 64 to 127, ...) at most 5 rows name the same one
- route_weights: float32 [16384, 2], P(('sp', 'tp')), may hold values from 0.25 to 2.5
- expert_gate: bfloat16 [32, 2048, 3072], P('sp', None, 'tp'), may hold values from -0.125 to 0.125
- expert_up: bfloat16 [32, 2048, 3072], P('sp', None, 'tp'), may hold values from -0.125 to 0.125
- expert_down: bfloat16 [32, 3072, 2048], P('sp', 'tp'), may hold values from -0.109375 to 0.109375
- shared_gate: bfloat16 [2048, 256], replicated, may hold values from -0.125 to 0.125
- shared_up: bfloat16 [2048, 256], replicated, may hold values from -0.125 to 0.125
- shared_down: bfloat16 [256, 2048], replicated, may hold values from -0.375 to 0.375
- second_gain: float32 [2048], replicated, may hold values from 0.1 to 1.9
- second_bias: float32 [2048], replicated, may hold values from -1.8 to 1.8
Outputs:
- layer_output: bfloat16 [16384, 2048], P(('sp', 'tp'))
Inputs may be any that keep to these rules, and one draw needn't show every extreme that they name: `route_ids`: each row names 2 different experts. The rows of one device (aligned blocks of 64 rows) name each expert at most 5 times, and in every draw some expert is named exactly 5 times in the rows of some device.
All inputs are finite; a program needn't handle non-finite values.
Results may differ from a plain program's by a relative error of at most 0.02.
The roundings to bfloat16 on the way count: a program that leaves them out, or rounds other values in their place, can miss the bound.
Values may be sent and summed in bfloat16 or wider, within the bound.
A program may use at most 128 MiB of HBM per device.

v0:
```python
import jax
import jax.numpy as jnp
from jax import lax
from jax.sharding import PartitionSpec as P

WIDE_HEADS = 16
WIDE_GROUPS = 4
NARROW_HEADS = 32
NARROW_GROUPS = 8
GRID_WIDTH = 64
SEQ_SHARDS = 4
LOCAL_EXPERTS = 2


EPS_HEAD = 1e-06
EPS_LAYER = 1e-05
ALPHA = 2.0**0.25
THETA = 10000.0


def swapped(x, axis, apart):
    return lax.ppermute(x, axis, [(i, i ^ 1 << apart) for i in range(lax.axis_size(axis))])


def head_norm(values, gain_vec):
    mean_square = jnp.mean(values * values, axis=-1, keepdims=True)
    return values * lax.rsqrt(mean_square + EPS_HEAD) * gain_vec


def rotate(values, position):
    half_size = values.shape[-1] // 2
    frequency = THETA ** (-jnp.arange(half_size, dtype=jnp.float32) / half_size)
    angles = position.astype(jnp.float32)[:, None] * frequency
    cosine = jnp.cos(angles)[:, None, :]
    sine_part = jnp.sin(angles)[:, None, :]
    leading = values[..., :half_size]
    trailing = values[..., half_size:]
    return jnp.concatenate(
        [leading * cosine - trailing * sine_part, trailing * cosine + leading * sine_part], axis=-1
    )


def grid_rotate(values, position):
    half_size = values.shape[-1] // 2
    grid_row = position // GRID_WIDTH
    grid_col = position % GRID_WIDTH
    return jnp.concatenate(
        [rotate(values[..., :half_size], grid_row), rotate(values[..., half_size:], grid_col)],
        axis=-1,
    )


def layer_norm(values, gain_vec, bias_vec):
    center = jnp.mean(values, axis=-1, keepdims=True)
    shifted = values - center
    variance = jnp.mean(shifted * shifted, axis=-1, keepdims=True)
    return (shifted * lax.rsqrt(variance + EPS_LAYER) * gain_vec + bias_vec).astype(jnp.bfloat16)


def prepare(queries, key_block, value_block, query_gain, key_gain, heads_total, groups, position):
    head_size = query_gain.shape[0]
    local_heads = queries.shape[1] // head_size
    group_index = lax.axis_index("tp") * local_heads // (heads_total // groups)
    query_rows = queries.reshape(queries.shape[0], local_heads, head_size).astype(jnp.float32)
    rotated_queries = grid_rotate(head_norm(query_rows, query_gain), position).astype(jnp.bfloat16)
    column_start = group_index * head_size
    key_rows = lax.dynamic_slice_in_dim(key_block, column_start, head_size, 1).astype(jnp.float32)[
        :, None, :
    ]
    rotated_keys = grid_rotate(head_norm(key_rows, key_gain), position)[:, 0, :].astype(
        jnp.bfloat16
    )
    value_rows = lax.dynamic_slice_in_dim(value_block, column_start, head_size, 1)
    return (rotated_queries, jnp.concatenate([rotated_keys, value_rows], axis=1))


def attend_local(rotated_queries, key_block, value_block):
    seg_rows, local_heads, head_size = rotated_queries.shape
    block_rows = min(512, seg_rows)
    score_scale = head_size ** (-0.5)
    blocks = rotated_queries.reshape(seg_rows // block_rows, block_rows, local_heads, head_size)

    def one_block(query_block):
        scores = (
            jnp.einsum("qhd,kd->hqk", query_block, key_block, preferred_element_type=jnp.float32)
            * score_scale
        )
        largest = jnp.max(scores, axis=-1, keepdims=True)
        weights = jnp.exp(scores - largest)
        weights = (weights / jnp.sum(weights, axis=-1, keepdims=True)).astype(jnp.bfloat16)
        return jnp.einsum(
            "hqk,kd->qhd", weights, value_block, preferred_element_type=jnp.float32
        ).astype(jnp.bfloat16)

    mixed_rows = lax.map(one_block, blocks)
    return mixed_rows.reshape(seg_rows, local_heads * head_size)


def local(
    residual,
    wide_query,
    narrow_query,
    wide_keys,
    narrow_keys,
    wide_values,
    narrow_values,
    wide_query_gain,
    wide_key_gain,
    narrow_query_gain,
    narrow_key_gain,
    wide_out,
    narrow_out,
    first_gain,
    first_bias,
    route_ids,
    route_weights,
    expert_gate,
    expert_up,
    expert_down,
    shared_gate,
    shared_up,
    shared_down,
    second_gain,
    second_bias,
):
    seg_rows = wide_query.shape[0]
    position = lax.axis_index("sp") % SEQ_SHARDS * seg_rows + jnp.arange(seg_rows, dtype=jnp.int32)
    wide_rotated, wide_pack = prepare(
        wide_query,
        wide_keys,
        wide_values,
        wide_query_gain,
        wide_key_gain,
        WIDE_HEADS,
        WIDE_GROUPS,
        position,
    )
    narrow_rotated, narrow_pack = prepare(
        narrow_query,
        narrow_keys,
        narrow_values,
        narrow_query_gain,
        narrow_key_gain,
        NARROW_HEADS,
        NARROW_GROUPS,
        position,
    )
    gathered = jnp.concatenate([wide_pack, narrow_pack], axis=1)
    for level in range(SEQ_SHARDS.bit_length() - 1):
        partner = swapped(gathered, "sp", level)
        is_upper = lax.axis_index("sp") // 2**level % 2 == 1
        gathered = jnp.where(
            is_upper,
            jnp.concatenate([partner, gathered], axis=0),
            jnp.concatenate([gathered, partner], axis=0),
        )
    wide_size = wide_query_gain.shape[0]
    narrow_size = narrow_query_gain.shape[0]
    narrow_start = 2 * wide_size
    wide_mixed = attend_local(
        wide_rotated, gathered[:, :wide_size], gathered[:, wide_size:narrow_start]
    )
    narrow_mixed = attend_local(
        narrow_rotated,
        gathered[:, narrow_start : narrow_start + narrow_size],
        gathered[:, narrow_start + narrow_size :],
    )
    wide_tokens, narrow_tokens = (
        lax.all_to_all(wide_mixed, "tp", split_axis=0, concat_axis=1, tiled=True),
        lax.all_to_all(narrow_mixed, "tp", split_axis=0, concat_axis=1, tiled=True),
    )
    running = jnp.dot(
        wide_tokens,
        lax.all_gather(wide_out, "tp", axis=0, tiled=True),
        preferred_element_type=jnp.float32,
    )
    projected = running + jnp.dot(
        narrow_tokens,
        lax.all_gather(narrow_out, "tp", axis=0, tiled=True),
        preferred_element_type=jnp.float32,
    )
    hidden = layer_norm(ALPHA * residual.astype(jnp.float32) + projected, first_gain, first_bias)
    device_rows = hidden.shape[0]
    model_width = hidden.shape[1]
    sp_size = lax.axis_size("sp")
    top_count = route_ids.shape[1]
    experts = LOCAL_EXPERTS * sp_size
    capacity = max(2, (5 * device_rows * top_count + 4 * experts - 1) // (4 * experts))
    flat_ids = route_ids.reshape(-1)
    expert_hits = (flat_ids[:, None] == jnp.arange(experts, dtype=jnp.int32)[None, :]).astype(
        jnp.int32
    )
    earlier = jnp.sum((jnp.cumsum(expert_hits, axis=0) - expert_hits) * expert_hits, axis=1)
    slot_index = flat_ids * capacity + earlier
    chosen = (
        slot_index[:, None] == jnp.arange(experts * capacity, dtype=jnp.int32)[None, :]
    ).astype(jnp.float32)
    chosen = chosen.reshape(device_rows, top_count, experts * capacity)
    placing = jnp.sum(chosen, axis=1).astype(jnp.bfloat16)
    mixing = jnp.sum(chosen * route_weights[:, :, None], axis=1)
    outgoing = jnp.einsum("rs,rd->sd", placing, hidden, preferred_element_type=jnp.float32).astype(
        jnp.bfloat16
    )
    outgoing = outgoing.reshape(sp_size, LOCAL_EXPERTS, capacity, model_width)
    piece_rows = lax.all_gather(
        lax.all_to_all(outgoing, "sp", split_axis=0, concat_axis=0, tiled=True),
        "tp",
        axis=0,
        tiled=True,
    )
    gate_values = jnp.einsum(
        "secd,edf->secf", piece_rows, expert_gate, preferred_element_type=jnp.float32
    )
    up_values = jnp.einsum(
        "secd,edf->secf", piece_rows, expert_up, preferred_element_type=jnp.float32
    )
    active = (jax.nn.silu(gate_values) * up_values).astype(jnp.bfloat16)
    partial_value = jnp.einsum(
        "secf,efd->secd", active, expert_down, preferred_element_type=jnp.float32
    )
    rounded = lax.optimization_barrier(partial_value.astype(jnp.bfloat16))
    partials = rounded.astype(jnp.float32)
    summed = lax.psum_scatter(partials.astype(jnp.bfloat16), "tp", scatter_dimension=0, tiled=True)
    returned = lax.all_to_all(summed, "sp", split_axis=0, concat_axis=0, tiled=True)
    routed = jnp.dot(mixing, returned.reshape(-1, model_width).astype(jnp.float32))
    shared_gate_values = jnp.dot(hidden, shared_gate, preferred_element_type=jnp.float32)
    shared_up_values = jnp.dot(hidden, shared_up, preferred_element_type=jnp.float32)
    shared_active = (jax.nn.silu(shared_gate_values) * shared_up_values).astype(jnp.bfloat16)
    shared_output = jnp.dot(shared_active, shared_down, preferred_element_type=jnp.float32)
    return layer_norm(
        ALPHA * hidden.astype(jnp.float32) + routed + shared_output, second_gain, second_bias
    )


def solution(mesh):
    in_specs = (
        P(("sp", "tp"), None),
        P("sp", "tp"),
        P("sp", "tp"),
        P("sp", None),
        P("sp", None),
        P("sp", None),
        P("sp", None),
        P(),
        P(),
        P(),
        P(),
        P("tp", None),
        P("tp", None),
        P(),
        P(),
        P(("sp", "tp"), None),
        P(("sp", "tp"), None),
        P("sp", None, "tp"),
        P("sp", None, "tp"),
        P("sp", "tp", None),
        P(),
        P(),
        P(),
        P(),
        P(),
    )
    out_specs = P(("sp", "tp"), None)
    return jax.shard_map(local, mesh=mesh, in_specs=in_specs, out_specs=out_specs, check_vma=False)
```

profile of v0, /device:TPU:1, one launch (start us, length us, event | category | flops | bytes accessed | tf_op | source)
XLA Modules:
  0.0 330.2 jit_solution(2909898347180493930)
XLA Ops:
  12.6 2.1 collective-permute-start
  15.7 6.6 %collective-permute-done = bf16[1024,192]{0,1:T(8,128)(2,1)} collective-permute-done((bf16[1024,192]{0,1:T(8,128)(2,1)S(1)}, bf16[1024,192]{0,1:T(8,128)(2,1)}, u32[]{:S(2)}, u32[]{:S(2)}) %collective-permute-start) | collective-permute-done | bytes 393248 | tf_op jit(solution)/shard_map/ppermute | solution.py:22
  22.3 1.4 maximum_select_fusion.1
  23.6 4.2 %collective-permute-start.1 = (bf16[2048,192]{0,1:T(8,128)(2,1)S(1)}, bf16[2048,192]{0,1:T(8,128)(2,1)S(1)}, u32[]{:S(2)}, u32[]{:S(2)}) collective-permute-start(bf16[2048,192]{0,1:T(8,128)(2,1)S(1)} %maximum_select_fusion.1), channel_id=1, source_target_pairs={{0,32},{16,48},{32,0},{48,16},{64,96},{80,112},{96,64},{112,80},{1... | collective-permute-start | bytes 2359304 | tf_op jit(solution)/shard_map/ppermute | solution.py:22
  33.4 10.5 %collective-permute-done.1 = bf16[2048,192]{0,1:T(8,128)(2,1)S(1)} collective-permute-done((bf16[2048,192]{0,1:T(8,128)(2,1)S(1)}, bf16[2048,192]{0,1:T(8,128)(2,1)S(1)}, u32[]{:S(2)}, u32[]{:S(2)}) %collective-permute-start.1) | collective-permute-done | bytes 786464 | tf_op jit(solution)/shard_map/ppermute | solution.py:22
  45.9 1.5 copy.143
  48.7 10.7 %while.20 = (s32[]{:T(128)}, bf16[2,512,1,64]{1,3,2,0:T(8,128)(2,1)S(1)}, bf16[2,512,1,64]{1,3,2,0:T(8,128)(2,1)S(1)}, bf16[4096,64]{1,0:T(8,128)(2,1)S(1)}, bf16[4096,64]{1,0:T(8,128)(2,1)}, /*index=5*/s32[]{:T(128)}) while((s32[]{:T(128)}, bf16[2,512,1,64]{1,3,2,0:T(8,128)(2,1)S(1)}, bf16[2,512,1,64]{1,3,2,0:T(8,128)(2,1)S(1)}, ...), condition=%wide.region_6.7_spmd, body=%wide.region_3.6_spmd.sunk | while | flops 555777024 | bytes 29501552 | solution.py:95
  48.7 1.4 multiply_reduce_fusion.4
  50.1 1.5 fusion.220
  51.6 2.4 fusion.221
  54.1 1.4 multiply_reduce_fusion.4
  55.5 1.5 fusion.220
  57.0 2.4 fusion.221
  60.8 11.1 %all-to-all-start = ((bf16[16,2,2048]{2,1,0:T(2,128)(2,1)}), bf16[16,2,2048]{2,1,0:T(2,128)(2,1)S(1)}, u32[]{:S(2)}, u32[]{:S(2)}) async-start(bf16[16,2,2048]{2,1,0:T(2,128)(2,1)} %reshape.649), calls=%async_computation | async-start | bytes 262144 | tf_op jit(solution)/shard_map/all_to_all | solution.py:169
  73.0 23.8 %while.21 = (s32[]{:T(128)}, bf16[2,512,2,32]{1,3,2,0:T(8,128)(2,1)S(1)}, bf16[2,512,2,32]{1,3,2,0:T(8,128)(2,1)S(1)}, bf16[4096,32]{0,1:T(8,128)(2,1)S(1)}, bf16[4096,32]{0,1:T(8,128)(2,1)S(1)}, /*index=5*/s32[]{:T(128)}) while((s32[]{:T(128)}, bf16[2,512,2,32]{1,3,2,0:T(8,128)(2,1)S(1)}, bf16[2,512,2,32]{1,3,2,0:T(8,128)(2,1)S(1)}, ...), condition=%wide.region_11.12_spmd, body=%wide.region_8.11_spmd.sunk | while | flops 834708480 | bytes 992337 | solution.py:95
  73.0 5.9 %fusion.228 = f32[2,512]{1,0:T(2,128)S(1)} fusion(bf16[4096,32]{0,1:T(8,128)(2,1)S(1)} %get-tuple-element.287, bf16[2,512,2,32]{1,3,2,0:T(8,128)(2,1)S(1)} %get-tuple-element.286, s32[]{:T(128)S(6)} %copy.193), kind=kOutput, calls=%fused_computation.205.clone.1 | convolution fusion | flops 281022464 | bytes 331780 | tf_op jit(solution)/shard_map/while/body/eval_jaxpr/sub | solution.py:89
  78.9 6.0 %fusion.229 = bf16[2,512,2,32]{1,3,2,0:T(8,128)(2,1)S(1)} fusion(bf16[2,512,2,32]{1,3,2,0:T(8,128)(2,1)S(1)} %get-tuple-element.279, s32[]{:T(128)S(6)} %copy.193, f32[2,512]{1,0:T(2,128)S(1)} %fusion.228, bf16[4096,32]{0,1:T(8,128)(2,1)S(1)} %get-tuple-element.288, bf16[4096,32]{0,1:T(8,128)(2,1)S(1)} %get-tuple-element.287, ...), kind=kOutput, calls=%fused_computation.28.clone.1 | convolution fusion | flops 553686016 | bytes 660480 | tf_op jit(solution)/shard_map/while/body/eval_jaxpr/hqk,kd->qhd/dot_general | solution.py:91
  84.9 5.9 %fusion.228 = f32[2,512]{1,0:T(2,128)S(1)} fusion(bf16[4096,32]{0,1:T(8,128)(2,1)S(1)} %get-tuple-element.287, bf16[2,512,2,32]{1,3,2,0:T(8,128)(2,1)S(1)} %get-tuple-element.286, s32[]{:T(128)S(6)} %copy.193), kind=kOutput, calls=%fused_computation.205.clone.1 | convolution fusion | flops 281022464 | bytes 331780 | tf_op jit(solution)/shard_map/while/body/eval_jaxpr/sub | solution.py:89
  90.8 6.0 %fusion.229 = bf16[2,512,2,32]{1,3,2,0:T(8,128)(2,1)S(1)} fusion(bf16[2,512,2,32]{1,3,2,0:T(8,128)(2,1)S(1)} %get-tuple-element.279, s32[]{:T(128)S(6)} %copy.193, f32[2,512]{1,0:T(2,128)S(1)} %fusion.228, bf16[4096,32]{0,1:T(8,128)(2,1)S(1)} %get-tuple-element.288, bf16[4096,32]{0,1:T(8,128)(2,1)S(1)} %get-tuple-element.287, ...), kind=kOutput, calls=%fused_computation.28.clone.1 | convolution fusion | flops 553686016 | bytes 660480 | tf_op jit(solution)/shard_map/while/body/eval_jaxpr/hqk,kd->qhd/dot_general | solution.py:91
  98.1 7.4 %all-to-all-start.1 = ((bf16[16,2,2048]{2,1,0:T(2,128)(2,1)}), bf16[16,2,2048]{2,1,0:T(2,128)(2,1)S(1)}, u32[]{:S(2)}, u32[]{:S(2)}) async-start(bf16[16,2,2048]{2,1,0:T(2,128)(2,1)} %reshape.651), calls=%async_computation.1 | async-start | bytes 262144 | tf_op jit(solution)/shard_map/all_to_all | solution.py:170
  106.7 7.7 %all-to-all-done.1 = bf16[16,2,2048]{2,1,0:T(2,128)(2,1)S(1)} async-done(((bf16[16,2,2048]{2,1,0:T(2,128)(2,1)}), bf16[16,2,2048]{2,1,0:T(2,128)(2,1)S(1)}, u32[]{:S(2)}, u32[]{:S(2)}) %all-to-all-start.1) | async-done | bytes 131104 | tf_op jit(solution)/shard_map/all_to_all | solution.py:170
  114.6 3.1 fusion.185
  117.8 3.2 fusion.183
  122.8 19.6 %all_to_all.48 = bf16[16,2,5,2048]{3,1,2,0:T(2,128)(2,1)S(1)} all-to-all(bf16[16,2,5,2048]{3,1,2,0:T(2,128)(2,1)S(1)} %copy.154), channel_id=1, replica_groups=mesh['sp'=16,'tp'=16] {'sp'}, dimensions={0} | all-to-all | bytes 1310720 | tf_op jit(solution)/shard_map/all_to_all | solution.py:206
  143.5 59.8 %all-gather.8.cloned.1.call-done = bf16[256,2,5,2048]{3,0,2,1:T(8,128)(2,1)} async-done(((bf16[16,2,5,2048]{3,0,2,1:T(8,128)(2,1)}), bf16[256,2,5,2048]{3,0,2,1:T(8,128)(2,1)}) %all-gather.8.cloned.1.call-update) | async-done | bytes 10485776 | tf_op jit(solution)/shard_map/all_gather | solution.py:205
  203.2 8.9 %fusion.90 = f32[2,256,5,192]{1,3,2,0:T(8,128)} fusion(bf16[256,2,5,2048]{3,0,2,1:T(8,128)(2,1)} %all-gather.8.cloned.1.call-done, bf16[2,2048,192]{1,2,0:T(8,128)(2,1)S(1)} %copy-done.2), kind=kOutput, calls=%fused_computation.58 | convolution fusion | flops 2013265920 | bytes 14024704 | tf_op jit(solution)/shard_map/secd,edf->secf/dot_general | solution.py:214
  212.1 17.2 %convert_bitcast_fusion = bf16[256,2,5,2048]{3,0,2,1:T(8,128)(2,1)} fusion(f32[2,256,5,192]{1,3,2,0:T(8,128)} %fusion.90, bf16[256,2,5,2048]{3,0,2,1:T(8,128)(2,1)} %all-gather.8.cloned.1.call-done, bf16[2,192,2048]{2,1,0:T(8,128)(2,1)S(1)} %copy-done, bf16[2,2048,192]{1,2,0:T(8,128)(2,1)} %param.46), kind=kOutput, calls=%fused_computation.43 | convolution fusion | flops 4034723840 | bytes 26083328 | tf_op jit(solution)/shard_map/secf,efd->secd/dot_general | solution.py:218
  229.4 70.3 %reduce-scatter.2.cloned.1.call-done = bf16[16,2,5,2048]{3,0,2,1:T(8,128)(2,1)} async-done(((bf16[256,2,5,2048]{3,0,2,1:T(8,128)(2,1)}), bf16[16,2,5,2048]{3,0,2,1:T(8,128)(2,1)}) %reduce-scatter.2.cloned.1.call-update) | async-done | bytes 655376 | tf_op jit(solution)/shard_map/reduce_scatter | solution.py:223
  299.6 2.6 copy.156
  302.2 6.5 %all-to-all-start.3 = ((bf16[16,2,5,2048]{3,1,2,0:T(2,128)(2,1)}), bf16[16,2,5,2048]{3,1,2,0:T(2,128)(2,1)S(1)}, u32[]{:S(2)}, u32[]{:S(2)}) async-start(bf16[16,2,5,2048]{3,1,2,0:T(2,128)(2,1)} %copy.156), calls=%async_computation.4 | async-start | bytes 1310720 | tf_op jit(solution)/shard_map/all_to_all | solution.py:224
  309.7 8.8 %all-to-all-done.3 = bf16[16,2,5,2048]{3,1,2,0:T(2,128)(2,1)S(1)} async-done(((bf16[16,2,5,2048]{3,1,2,0:T(2,128)(2,1)}), bf16[16,2,5,2048]{3,1,2,0:T(2,128)(2,1)S(1)}, u32[]{:S(2)}, u32[]{:S(2)}) %all-to-all-start.3) | async-done | bytes 655392 | tf_op jit(solution)/shard_map/all_to_all | solution.py:224
  320.1 2.5 fusion.184
  (137 shorter events, 27.2 us)
Async XLA Ops:
  6.5 205.6 %copy-start = (bf16[2,192,2048]{2,1,0:T(8,128)(2,1)S(1)}, bf16[2,192,2048]{2,1,0:T(8,128)(2,1)}, u32[]{:S(2)}) copy-start(bf16[2,192,2048]{2,1,0:T(8,128)(2,1)} %param.48) | copy-start | bytes 4718596
  6.5 4.0 %copy-start.19 = (f32[32]{0:T(128)S(1)}, f32[32]{0:T(128)}, u32[]{:S(2)}) copy-start(f32[32]{0:T(128)} %param.39) | copy-start | bytes 388
  6.5 4.4 %copy-start.5 = (bf16[1024,64]{0,1:T(8,128)(2,1)S(1)}, bf16[1024,64]{0,1:T(8,128)(2,1)}, u32[]{:S(2)}) copy-start(bf16[1024,64]{0,1:T(8,128)(2,1)} %param.30) | copy-start | bytes 393220
  6.5 4.6 %copy-start.20 = (f32[64]{0:T(128)S(1)}, f32[64]{0:T(128)}, u32[]{:S(2)}) copy-start(f32[64]{0:T(128)} %param.36) | copy-start | bytes 772
  6.5 4.7 %copy-start.21 = (f32[64]{0:T(128)S(1)}, f32[64]{0:T(128)}, u32[]{:S(2)}) copy-start(f32[64]{0:T(128)} %param.37) | copy-start | bytes 772
  6.5 108.1 %all-gather.4.cloned.1.call-start = ((), (), s32[]{:S(2)}) async-start(), calls=%async_computation.5 | async-start | bytes 4456448 | tf_op jit(solution)/shard_map/all_gather | solution.py:174
  7.3 110.4 %all-gather.6.cloned.1.call-start = ((), (), s32[]{:S(2)}) async-start(), calls=%async_computation.6 | async-start | bytes 4456448 | tf_op jit(solution)/shard_map/all_gather | solution.py:179
  8.6 6.1 %copy-start.15 = (s32[64,2]{0,1:T(2,128)S(1)}, s32[64,2]{0,1:T(2,128)}, u32[]{:S(2)}) copy-start(s32[64,2]{0,1:T(2,128)} %param.44) | copy-start | bytes 1540
  8.8 6.5 %copy-start.6 = (bf16[1024,64]{0,1:T(8,128)(2,1)S(1)}, bf16[1024,64]{0,1:T(8,128)(2,1)}, u32[]{:S(2)}) copy-start(bf16[1024,64]{0,1:T(8,128)(2,1)} %param.31) | copy-start | bytes 393220
  12.6 9.7 %collective-permute-start = (bf16[1024,192]{0,1:T(8,128)(2,1)S(1)}, bf16[1024,192]{0,1:T(8,128)(2,1)}, u32[]{:S(2)}, u32[]{:S(2)}) collective-permute-start(bf16[1024,192]{0,1:T(8,128)(2,1)S(1)} %pad_maximum_fusion), channel_id=1, source_target_pairs={{0,16},{16,0},{32,48},{48,32},{64,80},{80,64},{96,112},{112,96},{1... | collective-permute-start | bytes 1179656 | tf_op jit(solution)/shard_map/ppermute | solution.py:22
  23.6 20.3 %collective-permute-start.1 = (bf16[2048,192]{0,1:T(8,128)(2,1)S(1)}, bf16[2048,192]{0,1:T(8,128)(2,1)S(1)}, u32[]{:S(2)}, u32[]{:S(2)}) collective-permute-start(bf16[2048,192]{0,1:T(8,128)(2,1)S(1)} %maximum_select_fusion.1), channel_id=1, source_target_pairs={{0,32},{16,48},{32,0},{48,16},{64,96},{80,112},{96,64},{112,80},{1... | collective-permute-start | bytes 2359304 | tf_op jit(solution)/shard_map/ppermute | solution.py:22
  44.5 1.4 copy-start.1
  44.5 4.3 %copy-start.9 = (bf16[2,512,1,64]{1,3,2,0:T(8,128)(2,1)S(1)}, bf16[2,512,1,64]{1,3,2,0:T(8,128)(2,1)}, u32[]{:S(2)}) copy-start(bf16[2,512,1,64]{1,3,2,0:T(8,128)(2,1)} %custom-call) | copy-start | bytes 393220
  48.7 24.2 %copy-start.8 = (bf16[2,512,2,32]{1,3,2,0:T(8,128)(2,1)S(1)}, bf16[2,512,2,32]{1,3,2,0:T(8,128)(2,1)}, u32[]{:S(2)}) copy-start(bf16[2,512,2,32]{1,3,2,0:T(8,128)(2,1)} %custom-call.1) | copy-start | bytes 393220
  50.1 1.5 copy-start.3
  55.5 1.5 copy-start.3
  60.8 37.3 %all-to-all-start = ((bf16[16,2,2048]{2,1,0:T(2,128)(2,1)}), bf16[16,2,2048]{2,1,0:T(2,128)(2,1)S(1)}, u32[]{:S(2)}, u32[]{:S(2)}) async-start(bf16[16,2,2048]{2,1,0:T(2,128)(2,1)} %reshape.649), calls=%async_computation | async-start | bytes 262144 | tf_op jit(solution)/shard_map/all_to_all | solution.py:169
  73.0 32.8 %copy-start.16 = (s32[64,2]{0,1:T(2,128)S(1)}, s32[64,2]{0,1:T(2,128)}, u32[]{:S(2)}) copy-start(s32[64,2]{0,1:T(2,128)} %param.44) | copy-start | bytes 1540
  73.0 32.8 %copy-start.17 = (s32[64,2]{0,1:T(2,128)S(1)}, s32[64,2]{0,1:T(2,128)}, u32[]{:S(2)}) copy-start(s32[64,2]{0,1:T(2,128)} %copy.153) | copy-start | bytes 1540
  73.0 32.8 %copy-start.18 = (f32[64,2]{0,1:T(2,128)S(1)}, f32[64,2]{0,1:T(2,128)}, u32[]{:S(2)}) copy-start(f32[64,2]{0,1:T(2,128)} %param.45) | copy-start | bytes 1540
  98.1 19.6 %copy-start.7 = (bf16[64,2048]{1,0:T(8,128)(2,1)S(1)}, bf16[64,2048]{1,0:T(8,128)(2,1)}, u32[]{:S(2)}) copy-start(bf16[64,2048]{1,0:T(8,128)(2,1)} %param.29) | copy-start | bytes 786436
  98.1 16.2 %all-to-all-start.1 = ((bf16[16,2,2048]{2,1,0:T(2,128)(2,1)}), bf16[16,2,2048]{2,1,0:T(2,128)(2,1)S(1)}, u32[]{:S(2)}, u32[]{:S(2)}) async-start(bf16[16,2,2048]{2,1,0:T(2,128)(2,1)} %reshape.651), calls=%async_computation.1 | async-start | bytes 262144 | tf_op jit(solution)/shard_map/all_to_all | solution.py:170
  105.5 97.8 %all-gather.8.cloned.1.call-start = ((), (), s32[]{:S(2)}) async-start(), calls=%async_computation.7 | async-start | bytes 11141120 | tf_op jit(solution)/shard_map/all_gather | solution.py:205
  117.7 3.5 %copy-start.11 = (f32[2048]{0:T(1024)S(1)}, f32[2048]{0:T(1024)}, u32[]{:S(2)}) copy-start(f32[2048]{0:T(1024)} %param.43) | copy-start | bytes 24580
  117.7 3.5 %copy-start.12 = (f32[2048]{0:T(1024)S(1)}, f32[2048]{0:T(1024)}, u32[]{:S(2)}) copy-start(f32[2048]{0:T(1024)} %param.42) | copy-start | bytes 24580
  117.7 3.6 %copy-start.10 = (bf16[64,160]{1,0:T(8,128)(2,1)S(1)}, bf16[64,160]{1,0:T(8,128)(2,1)}, u32[]{:S(2)}) copy-start(bf16[64,160]{1,0:T(8,128)(2,1)} %get-tuple-element.116) | copy-start | bytes 61444
  122.7 80.5 %copy-start.2 = (bf16[2,2048,192]{1,2,0:T(8,128)(2,1)S(1)}, bf16[2,2048,192]{1,2,0:T(8,128)(2,1)}, u32[]{:S(2)}) copy-start(bf16[2,2048,192]{1,2,0:T(8,128)(2,1)} %param.47) | copy-start | bytes 4718596
  143.4 156.2 %reduce-scatter.2.cloned.1.call-start = ((), (), s32[]{:S(2)}) async-start(), calls=%async_computation.8 | async-start | bytes 11141120 | tf_op jit(solution)/shard_map/reduce_scatter | solution.py:223
  229.3 79.4 %copy-start.4 = (bf16[2048,256]{1,0:T(8,128)(2,1)S(1)}, bf16[2048,256]{1,0:T(8,128)(2,1)}, u32[]{:S(2)}) copy-start(bf16[2048,256]{1,0:T(8,128)(2,1)} %param.49) | copy-start | bytes 3145732
  302.2 16.2 %all-to-all-start.3 = ((bf16[16,2,5,2048]{3,1,2,0:T(2,128)(2,1)}), bf16[16,2,5,2048]{3,1,2,0:T(2,128)(2,1)S(1)}, u32[]{:S(2)}, u32[]{:S(2)}) async-start(bf16[16,2,5,2048]{3,1,2,0:T(2,128)(2,1)} %copy.156), calls=%async_computation.4 | async-start | bytes 1310720 | tf_op jit(solution)/shard_map/all_to_all | solution.py:224
  319.0 3.8 %copy-start.13 = (f32[2048]{0:T(1024)S(1)}, f32[2048]{0:T(1024)}, u32[]{:S(2)}) copy-start(f32[2048]{0:T(1024)} %param.53) | copy-start | bytes 24580
  319.0 3.8 %copy-start.14 = (f32[2048]{0:T(1024)S(1)}, f32[2048]{0:T(1024)}, u32[]{:S(2)}) copy-start(f32[2048]{0:T(1024)} %param.52) | copy-start | bytes 24580
Sparse Core Ops, SparseCore 0:
  9.2 46.0 all-gather.3
  57.1 42.5 all-gather.5
  143.5 59.6 all-gather.7
  229.5 70.0 reduce-scatter.1
where the time goes:
time: 333 us; the launch traced here: 330 us
  waiting for transfers between devices  164 us (49%)
  matrix products  68.5 us (21%)
  starting transfers between devices  31.6 us (9%)
  local copies, waits for them, and re-layouts  20.5 us (6%)
  blocking collectives  19.6 us (6%)
  between operations  13.9 us (4%)
  other arithmetic  11.7 us (4%)
    reduce_scatter x1, waiting for transfers between devices, local(): lax.psum_scatter(partials.astype(jnp.bfloat16), 'tp', scatter_dimension=0...  70.3 us
    all_gather x1, waiting for transfers between devices, local(): lax.all_gather(lax.all_to_all(outgoing, 'sp', split_axis=0, concat_axis=0...  59.8 us
    all_to_all x1, blocking collectives, local(): lax.all_to_all(outgoing, 'sp', split_axis=0, concat_axis=0, tiled=True)  19.6 us
    dot_general x1, matrix products, local(): jnp.einsum('secf,efd->secd', active, expert_down, preferred_element_type=...  17.2 us
    ppermute x2, waiting for transfers between devices, swapped(): lax.ppermute(x, axis, [(i, i ^ 1 << apart) for i in range(lax.axis_size(a...  17.1 us
    dot_general x4, matrix products, one_block(): jnp.einsum('hqk,kd->qhd', weights, value_block, preferred_element_type=jn...  16.9 us
    sub x2, matrix products, one_block(): weights = jnp.exp(scores - largest)  11.7 us
    all_to_all x1, starting transfers between devices, local(): lax.all_to_all(wide_mixed, 'tp', split_axis=0, concat_axis=1, tiled=True)  11.1 us
  transfers between devices with their start and end apart: 9, of which 6 were waited for; matrix products, arithmetic and copies ran while one was open for 18% of the time, Pallas kernels for 0%

commit v1 on v0

--- a/solution.py
+++ b/solution.py
@@ -1,6 +1,11 @@
+import functools
+
 import jax
 import jax.numpy as jnp
+import numpy as np
 from jax import lax
+from jax.experimental import pallas as pl
+from jax.experimental.pallas import tpu as pltpu
 from jax.sharding import PartitionSpec as P
 
 WIDE_HEADS = 16
@@ -181,54 +186,419 @@
     )
     hidden = layer_norm(ALPHA * residual.astype(jnp.float32) + projected, first_gain, first_bias)
     device_rows = hidden.shape[0]
-    model_width = hidden.shape[1]
     sp_size = lax.axis_size("sp")
     top_count = route_ids.shape[1]
     experts = LOCAL_EXPERTS * sp_size
-    capacity = max(2, (5 * device_rows * top_count + 4 * experts - 1) // (4 * experts))
     flat_ids = route_ids.reshape(-1)
     expert_hits = (flat_ids[:, None] == jnp.arange(experts, dtype=jnp.int32)[None, :]).astype(
         jnp.int32
     )
     earlier = jnp.sum((jnp.cumsum(expert_hits, axis=0) - expert_hits) * expert_hits, axis=1)
-    slot_index = flat_ids * capacity + earlier
+    slot_index = flat_ids * SLOT + earlier
     chosen = (
-        slot_index[:, None] == jnp.arange(experts * capacity, dtype=jnp.int32)[None, :]
+        slot_index[:, None] == jnp.arange(experts * SLOT, dtype=jnp.int32)[None, :]
     ).astype(jnp.float32)
-    chosen = chosen.reshape(device_rows, top_count, experts * capacity)
+    chosen = chosen.reshape(device_rows, top_count, experts * SLOT)
     placing = jnp.sum(chosen, axis=1).astype(jnp.bfloat16)
     mixing = jnp.sum(chosen * route_weights[:, :, None], axis=1)
     outgoing = jnp.einsum("rs,rd->sd", placing, hidden, preferred_element_type=jnp.float32).astype(
         jnp.bfloat16
     )
-    outgoing = outgoing.reshape(sp_size, LOCAL_EXPERTS, capacity, model_width)
-    piece_rows = lax.all_gather(
-        lax.all_to_all(outgoing, "sp", split_axis=0, concat_axis=0, tiled=True),
-        "tp",
-        axis=0,
-        tiled=True,
-    )
-    gate_values = jnp.einsum(
-        "secd,edf->secf", piece_rows, expert_gate, preferred_element_type=jnp.float32
-    )
-    up_values = jnp.einsum(
-        "secd,edf->secf", piece_rows, expert_up, preferred_element_type=jnp.float32
-    )
-    active = (jax.nn.silu(gate_values) * up_values).astype(jnp.bfloat16)
-    partial_value = jnp.einsum(
-        "secf,efd->secd", active, expert_down, preferred_element_type=jnp.float32
-    )
-    rounded = lax.optimization_barrier(partial_value.astype(jnp.bfloat16))
-    partials = rounded.astype(jnp.float32)
-    summed = lax.psum_scatter(partials.astype(jnp.bfloat16), "tp", scatter_dimension=0, tiled=True)
-    returned = lax.all_to_all(summed, "sp", split_axis=0, concat_axis=0, tiled=True)
-    routed = jnp.dot(mixing, returned.reshape(-1, model_width).astype(jnp.float32))
+    routed = moe(
+        outgoing,
+        mixing,
+        expert_gate,
+        expert_up,
+        expert_down,
+        sp_size,
+        lax.axis_size("tp") // 2,
+    )
     shared_gate_values = jnp.dot(hidden, shared_gate, preferred_element_type=jnp.float32)
     shared_up_values = jnp.dot(hidden, shared_up, preferred_element_type=jnp.float32)
     shared_active = (jax.nn.silu(shared_gate_values) * shared_up_values).astype(jnp.bfloat16)
     shared_output = jnp.dot(shared_active, shared_down, preferred_element_type=jnp.float32)
     return layer_norm(
         ALPHA * hidden.astype(jnp.float32) + routed + shared_output, second_gain, second_bias
+    )
+
+
+CAPACITY = 5
+SLOT = 8
+MESH = pl.DeviceIdType.MESH
+
+
+def moe_kernel(
+    n_sp,
+    n_z,
+    outgoing,
+    mixing,
+    pack,
+    spread,
+    gate_hbm,
+    up_hbm,
+    down_hbm,
+    routed,
+    arrived,
+    blocks,
+    sums,
+    landing,
+    sending,
+    returned,
+    gate_w,
+    up_w,
+    down_w,
+    hand_send,
+    hand_recv,
+    ring_send,
+    ring_recv,
+    sum_send,
+    sum_recv,
+    back_send,
+    back_recv,
+    own_sem,
+    pair_send,
+    pair_recv,
+):
+    half = n_z // 2
+    peers = 2 * n_sp
+    sp = lax.axis_index("sp")
+    tp = lax.axis_index("tp")
+    z = tp // 2
+    core = tp % 2
+    me = 2 * sp + core
+    right = (sp, 2 * ((z + 1) % n_z) + core)
+    left = (sp, 2 * ((z + n_z - 1) % n_z) + core)
+    partner = (sp, 2 * z + 1 - core)
+
+    def peer_id(index):
+        return (index // 2, 2 * z + index % 2)
+
+    def remote(src, dst, send_sem, recv_sem, device):
+        return pltpu.make_async_remote_copy(
+            src_ref=src,
+            dst_ref=dst,
+            send_sem=send_sem,
+            recv_sem=recv_sem,
+            device_id=device,
+            device_id_type=MESH,
+        )
+
+    own_copies = [
+        pltpu.make_async_copy(hbm.at[core], vmem.at[0], own_sem.at[i])
+        for i, (hbm, vmem) in enumerate(
+            ((gate_hbm, gate_w), (up_hbm, up_w), (down_hbm, down_w))
+        )
+    ]
+    for copy in own_copies:
+        copy.start()
+
+    barrier = pltpu.get_barrier_semaphore()
+
+    def greet(k, carry):
+        pl.semaphore_signal(
+            barrier, inc=1, device_id=peer_id((me + k) % peers), device_id_type=MESH
+        )
+        return carry
+
+    lax.fori_loop(1, peers, greet, 0)
+    for device in (left, right):
+        pl.semaphore_signal(barrier, inc=1, device_id=device, device_id_type=MESH)
+    pl.semaphore_wait(barrier, peers + 1)
+
+    def hand_copy(k):
+        g = (me + k) % peers
+        return remote(
+            outgoing.at[pl.ds(pl.multiple_of(SLOT * g, SLOT), SLOT)],
+            arrived.at[core, pl.ds(pl.multiple_of(SLOT * sp, SLOT), SLOT)],
+            hand_send.at[k],
+            hand_recv.at[k],
+            peer_id(g),
+        )
+
+    def hand_start(k, carry):
+        hand_copy(k).start()
+        return carry
+
+    lax.fori_loop(1, peers, hand_start, 0)
+    own_hand = pltpu.make_async_copy(
+        outgoing.at[pl.ds(pl.multiple_of(SLOT * me, SLOT), SLOT)],
+        arrived.at[core, pl.ds(pl.multiple_of(SLOT * sp, SLOT), SLOT)],
+        hand_recv.at[0],
+    )
+    own_hand.start()
+
+    pair_copies = [
+        remote(hbm.at[1 - core], vmem.at[1], pair_send.at[i], pair_recv.at[i], partner)
+        for i, (hbm, vmem) in enumerate(
+            ((gate_hbm, gate_w), (up_hbm, up_w), (down_hbm, down_w))
+        )
+    ]
+    for copy in pair_copies:
+        copy.start()
+
+    own_hand.wait()
+
+    def hand_wait(k, carry):
+        g = (me + peers - k) % peers
+        slot = arrived.at[g % 2, pl.ds(pl.multiple_of(SLOT * (g // 2), SLOT), SLOT)]
+        pltpu.make_async_remote_copy(
+            src_ref=outgoing.at[pl.ds(0, SLOT)],
+            dst_ref=slot,
+            send_sem=hand_send.at[k],
+            recv_sem=hand_recv.at[k],
+            device_id=peer_id(g),
+            device_id_type=MESH,
+        ).wait_recv()
+        return carry
+
+    lax.fori_loop(1, peers, hand_wait, 0)
+
+    def ring_copy(direction, hop, h):
+        block = (z + (n_z - hop + 1 if direction == 0 else hop - 1)) % n_z
+        return remote(
+            blocks.at[block, h],
+            blocks.at[block, h],
+            ring_send.at[direction, hop - 1, h],
+            ring_recv.at[direction, hop - 1, h],
+            right if direction == 0 else left,
+        )
+
+    def ring_arrival(direction, hop, h):
+        block = (z + (n_z - hop if direction == 0 else hop)) % n_z
+        return remote(
+            blocks.at[block, h],
+            blocks.at[block, h],
+            ring_send.at[direction, hop - 1, h],
+            ring_recv.at[direction, hop - 1, h],
+            right if direction == 0 else left,
+        )
+
+    for h in range(2):
+        blocks[z, h] = jnp.dot(
+            pack[...], arrived[h], preferred_element_type=jnp.float32
+        ).astype(jnp.bfloat16)
+        for direction in range(2):
+            if h == direction or half > 1:
+                ring_copy(direction, 1, h).start()
+
+    for copy in own_copies:
+        copy.wait()
+    for copy in pair_copies:
+        copy.wait()
+
+    def sum_send_first(direction):
+        block = (z + (half - 1 if direction == 0 else n_z - half + 1)) % n_z
+        return remote(
+            sums.at[block, direction],
+            landing.at[direction, 1, direction],
+            sum_send.at[direction, 1, direction],
+            sum_recv.at[direction, 1, direction],
+            right if direction == 0 else left,
+        )
+
+    def expert_step(i, carry):
+        hop = (i + 1) // 2
+
+        @pl.when(i % 2 == 1)
+        def _():
+            for first in range(2):
+                for direction in range(2):
+                    h = direction if first == 0 else 1 - direction
+                    limit = half if h == direction else half - 1
+
+                    @pl.when(hop <= limit)
+                    def _(direction=direction, h=h):
+                        ring_arrival(direction, hop, h).wait_recv()
+
+                    @pl.when(hop < limit)
+                    def _(direction=direction, h=h):
+                        ring_copy(direction, hop + 1, h).start()
+
+        block = (z + jnp.where(i % 2 == 1, n_z - hop, hop)) % n_z
+        rows = blocks[block].reshape(-1, blocks.shape[-1])
+        total = None
+        for side in range(2):
+            gate_values = jnp.dot(rows, gate_w[side], preferred_element_type=jnp.float32)
+            up_values = jnp.dot(rows, up_w[side], preferred_element_type=jnp.float32)
+            active = (gate_values / (1.0 + jnp.exp(-gate_values)) * up_values).astype(
+                jnp.bfloat16
+            )
+            part = jnp.dot(active, down_w[side], preferred_element_type=jnp.float32)
+            total = part if total is None else total + part
+        sums[block] = total.astype(jnp.bfloat16).reshape(sums.shape[1:])
+
+        @pl.when(i == n_z - 2)
+        def _():
+            for direction in range(2):
+                if half > 1:
+                    sum_send_first(direction).start()
+
+        return carry
+
+    lax.fori_loop(0, n_z, expert_step, 0)
+
+    def sum_copy(direction, step, h):
+        block = (
+            z + (half + 1 - step if direction == 0 else n_z - half - 1 + step)
+        ) % n_z
+        return block, remote(
+            sums.at[block, h],
+            landing.at[direction, step - 1, h],
+            sum_send.at[direction, step - 1, h],
+            sum_recv.at[direction, step - 1, h],
+            right if direction == 0 else left,
+        )
+
+    for direction in range(2):
+        sum_copy(direction, 1, 1 - direction)[1].start()
+    for step in range(2, half + 1):
+        for direction in range(2):
+            for h in (1 - direction, direction):
+                if h == direction and step == 2:
+                    continue
+                block, copy = sum_copy(direction, step, h)
+                sum_copy(direction, step - 1, h)[1].wait_recv()
+                sums[block, h] = (
+                    sums[block, h].astype(jnp.float32)
+                    + landing[direction, step - 2, h].astype(jnp.float32)
+                ).astype(jnp.bfloat16)
+                copy.start()
+
+    def back_copy(k):
+        g = (me + k) % peers
+        return remote(
+            sending.at[g % 2, pl.ds(pl.multiple_of(SLOT * (g // 2), SLOT), SLOT)],
+            returned.at[pl.ds(pl.multiple_of(SLOT * me, SLOT), SLOT)],
+            back_send.at[k],
+            back_recv.at[k],
+            peer_id(g),
+        )
+
+    for h in range(2):
+        total = sums[z, h].astype(jnp.float32)
+        for direction in range(2):
+            if h != direction or half > 1:
+                sum_copy(direction, half, h)[1].wait_recv()
+                total = total + landing[direction, half - 1, h].astype(jnp.float32)
+        sending[h] = jnp.dot(
+            spread[...], total.astype(jnp.bfloat16), preferred_element_type=jnp.float32
+        ).astype(jnp.bfloat16)
+
+        def back_start(j, carry, h=h):
+            k = 2 * j + (h + core) % 2
+
+            @pl.when(k > 0)
+            def _():
+                back_copy(k).start()
+
+            return carry
+
+        lax.fori_loop(0, n_sp, back_start, 0)
+
+    own_back = pltpu.make_async_copy(
+        sending.at[core, pl.ds(pl.multiple_of(SLOT * sp, SLOT), SLOT)],
+        returned.at[pl.ds(pl.multiple_of(SLOT * me, SLOT), SLOT)],
+        back_recv.at[0],
+    )
+    own_back.start()
+
+    for direction in range(2):
+        for hop in range(1, half + 1):
+            for h in range(2):
+                if hop <= (half if h == direction else half - 1):
+                    ring_copy(direction, hop, h).wait_send()
+                if hop > 1 or h != direction:
+                    sum_copy(direction, hop, h)[1].wait_send()
+
+    def hand_done(k, carry):
+        hand_copy(k).wait_send()
+        return carry
+
+    lax.fori_loop(1, peers, hand_done, 0)
+    own_back.wait()
+
+    def back_wait(k, carry):
+        g = (me + peers - k) % peers
+        pltpu.make_async_remote_copy(
+            src_ref=sending.at[0, pl.ds(0, SLOT)],
+            dst_ref=returned.at[pl.ds(pl.multiple_of(SLOT * g, SLOT), SLOT)],
+            send_sem=back_send.at[k],
+            recv_sem=back_recv.at[k],
+            device_id=peer_id(g),
+            device_id_type=MESH,
+        ).wait_recv()
+        return carry
+
+    lax.fori_loop(1, peers, back_wait, 0)
+
+    def back_done(k, carry):
+        back_copy(k).wait_send()
+        return carry
+
+    lax.fori_loop(1, peers, back_done, 0)
+
+    weights = mixing[...]
+    high = weights.astype(jnp.bfloat16)
+    low = (weights - high.astype(jnp.float32)).astype(jnp.bfloat16)
+    values = returned[...]
+    routed[...] = jnp.dot(high, values, preferred_element_type=jnp.float32) + jnp.dot(
+        low, values, preferred_element_type=jnp.float32
+    )
+
+
+def moe(outgoing, mixing, expert_gate, expert_up, expert_down, n_sp, n_z):
+    width = outgoing.shape[1]
+    hidden_units = expert_gate.shape[2]
+    half_rows = n_sp * CAPACITY
+    half = n_z // 2
+    row = np.arange(half_rows)
+    pack = np.zeros((half_rows, n_sp * SLOT), np.float32)
+    pack[row, SLOT * (row // CAPACITY) + row % CAPACITY] = 1.0
+    vmem = pl.BlockSpec(memory_space=pltpu.VMEM)
+    hbm = pl.BlockSpec(memory_space=pl.ANY)
+    dma = pltpu.SemaphoreType.DMA
+    bf16 = jnp.bfloat16
+    return pl.pallas_call(
+        functools.partial(moe_kernel, n_sp, n_z),
+        out_shape=jax.ShapeDtypeStruct((mixing.shape[0], width), jnp.float32),
+        in_specs=[vmem] * 4 + [hbm] * 3,
+        out_specs=vmem,
+        scratch_shapes=[
+            pltpu.VMEM((2, n_sp * SLOT, width), bf16),
+            pltpu.VMEM((n_z, 2, half_rows, width), bf16),
+            pltpu.VMEM((n_z, 2, half_rows, width), bf16),
+            pltpu.VMEM((2, half, 2, half_rows, width), bf16),
+            pltpu.VMEM((2, n_sp * SLOT, width), bf16),
+            pltpu.VMEM((2 * n_sp * SLOT, width), bf16),
+            pltpu.VMEM((2, width, hidden_units), bf16),
+            pltpu.VMEM((2, width, hidden_units), bf16),
+            pltpu.VMEM((2, hidden_units, width), bf16),
+            dma((2 * n_sp,)),
+            dma((2 * n_sp,)),
+            dma((2, half, 2)),
+            dma((2, half, 2)),
+            dma((2, half, 2)),
+            dma((2, half, 2)),
+            dma((2 * n_sp,)),
+            dma((2 * n_sp,)),
+            dma((3,)),
+            dma((3,)),
+            dma((3,)),
+        ],
+        compiler_params=pltpu.CompilerParams(
+            collective_id=0, has_side_effects=True, vmem_limit_bytes=56 * 2**20
+        ),
+        cost_estimate=pl.CostEstimate(
+            flops=6_000_000_000, bytes_accessed=10_000_000, transcendentals=1_000_000
+        ),
+    )(
+        outgoing,
+        mixing,
+        jnp.asarray(pack, bf16),
+        jnp.asarray(pack.T, bf16),
+        expert_gate,
+        expert_up,
+        expert_down,
     )
 
 

time: 333 us -> 283 us (0.85)
  waiting for transfers between devices: 164 us -> 13.3 us
  Pallas kernels: 0 us -> 139 us
  matrix products: 68.5 us -> 44.3 us
  blocking collectives: 19.6 us -> 0 us
  other arithmetic: 11.7 us -> 20.1 us
  starting transfers between devices: 31.6 us -> 23.9 us
  local copies, waits for them, and re-layouts: 20.5 us -> 27.1 us
    pallas_call x0 -> x1, Pallas kernels: none -> 139 us  [moe(): pl.pallas_call(functools.partial(moe_kernel, n_sp, n_z), out_shape=jax.Sh...]
    reduce_scatter x1 -> x0, waiting for transfers between devices: 70.3 us -> none  [local(): lax.psum_scatter(partials.astype(jnp.bfloat16), 'tp', scatter_dimension=0...]
    all_gather x1 -> x0, waiting for transfers between devices: 59.8 us -> none  [local(): lax.all_gather(lax.all_to_all(outgoing, 'sp', split_axis=0, concat_axis=0...]
    dot_general x3 -> x0, matrix products: 27.1 us -> none  [the longest x1 17.2 us: local(): jnp.einsum('secf,efd->secd', active, expert_down, preferred_element_type=...]
    all_to_all x1 -> x0, blocking collectives: 19.6 us -> none  [local(): lax.all_to_all(outgoing, 'sp', split_axis=0, concat_axis=0, tiled=True)]
    ppermute x2, waiting for transfers between devices: 17.1 us -> 4.57 us  [swapped(): lax.ppermute(x, axis, [(i, i ^ 1 << apart) for i in range(lax.axis_size(a...]
    all_to_all x1 -> x0, waiting for transfers between devices: 8.76 us -> none  [local(): lax.all_to_all(summed, 'sp', split_axis=0, concat_axis=0, tiled=True)]
    all_to_all x1, waiting for transfers between devices: 0.01 us -> 7.91 us  [local(): lax.all_to_all(wide_mixed, 'tp', split_axis=0, concat_axis=1, tiled=True)]
  transfers between devices with their start and end apart: 9 -> 6, of which waited for: 6 -> 2; matrix products, arithmetic and copies ran while one was open for 18% -> 29% of each run, Pallas kernels for 0% -> 0%
where the time goes in v1:
time: 283 us; the launch traced here: 282 us
  Pallas kernels  139 us (49%)
  matrix products  44.3 us (16%)
  local copies, waits for them, and re-layouts  27.1 us (10%)
  starting transfers between devices  23.9 us (8%)
  other arithmetic  20.1 us (7%)
  between operations  14 us (5%)
  waiting for transfers between devices  13.3 us (5%)
    pallas_call x1, Pallas kernels, moe(): pl.pallas_call(functools.partial(moe_kernel, n_sp, n_z), out_shape=jax.Sh...  139 us
    dot_general x4, matrix products, one_block(): jnp.einsum('hqk,kd->qhd', weights, value_block, preferred_element_type=jn...  18.2 us
    sub x2, matrix products, one_block(): weights = jnp.exp(scores - largest)  13.3 us
    all_to_all x1, starting transfers between devices, local(): lax.all_to_all(narrow_mixed, 'tp', split_axis=0, concat_axis=1, tiled=True)  10.2 us
    unnamed x43, local copies, waits for them, and re-layouts  9.05 us
    all_to_all x1, waiting for transfers between devices, local(): lax.all_to_all(wide_mixed, 'tp', split_axis=0, concat_axis=1, tiled=True)  7.91 us
    all_to_all x1, starting transfers between devices, local(): lax.all_to_all(wide_mixed, 'tp', split_axis=0, concat_axis=1, tiled=True)  7.23 us
    ppermute x2, starting transfers between devices, swapped(): lax.ppermute(x, axis, [(i, i ^ 1 << apart) for i in range(lax.axis_size(a...  6.45 us
  transfers between devices with their start and end apart: 6, of which 2 were waited for; matrix products, arithmetic and copies ran while one was open for 29% of the time, Pallas kernels for 0%

profile of v1, /device:TPU:1, one launch (start us, length us, event | category | flops | bytes accessed | tf_op | source)
XLA Modules:
  0.0 281.8 jit_solution(7379412828996253417)
XLA Ops:
  15.8 2.1 collective-permute-start
  20.9 4.6 %collective-permute-done = bf16[1024,192]{0,1:T(8,128)(2,1)} collective-permute-done((bf16[1024,192]{0,1:T(8,128)(2,1)S(1)}, bf16[1024,192]{0,1:T(8,128)(2,1)}, u32[]{:S(2)}, u32[]{:S(2)}) %collective-permute-start) | collective-permute-done | bytes 393248 | tf_op jit(solution)/shard_map/ppermute | solution.py:27
  25.5 1.6 maximum_select_fusion.1
  27.1 4.3 %collective-permute-start.1 = (bf16[2048,192]{0,1:T(8,128)(2,1)S(1)}, bf16[2048,192]{0,1:T(8,128)(2,1)}, u32[]{:S(2)}, u32[]{:S(2)}) collective-permute-start(bf16[2048,192]{0,1:T(8,128)(2,1)S(1)} %maximum_select_fusion.1), channel_id=1, source_target_pairs={{0,32},{16,48},{32,0},{48,16},{64,96},{80,112},{96,64},{112,80},{1... | collective-permute-start | bytes 2359304 | tf_op jit(solution)/shard_map/ppermute | solution.py:27
  36.0 1.4 copy.149
  37.4 1.4 copy.150
  38.7 1.4 copy.151
  41.5 2.4 copy.130.gate_hbm
  44.0 3.8 %copy.131.up_hbm = bf16[2,2048,192]{2,1,0:T(8,128)(2,1)} copy(bf16[2,2048,192]{1,2,0:T(8,128)(2,1)} %param.49) | data formatting | bytes 3145728 | tf_op args[18]
  48.6 1.9 maximum_select_fusion
  50.5 26.8 %while.21 = (s32[]{:T(128)}, bf16[2,512,2,32]{1,3,2,0:T(8,128)(2,1)}, bf16[2,512,2,32]{1,3,2,0:T(8,128)(2,1)}, bf16[4096,32]{0,1:T(8,128)(2,1)S(1)}, bf16[4096,32]{0,1:T(8,128)(2,1)S(1)}, /*index=5*/s32[]{:T(128)}) while((s32[]{:T(128)}, bf16[2,512,2,32]{1,3,2,0:T(8,128)(2,1)}, bf16[2,512,2,32]{1,3,2,0:T(8,128)(2,1)}, ...), condition=%wide.region_11.12_spmd, body=%wide.region_8.11_spmd.sunk | while | flops 834708480 | bytes 2565785 | solution.py:100
  50.6 6.7 %fusion.213 = f32[2,512]{1,0:T(2,128)S(1)} fusion(bf16[4096,32]{0,1:T(8,128)(2,1)S(1)} %get-tuple-element.277, bf16[2,512,2,32]{1,3,2,0:T(8,128)(2,1)} %get-tuple-element.276, s32[]{:T(128)} %get-tuple-element.268), kind=kOutput, calls=%fused_computation.190.clone.1 | convolution fusion | flops 281022464 | bytes 332288 | tf_op jit(solution)/shard_map/while/body/eval_jaxpr/sub | solution.py:94
  57.2 6.0 %fusion.214 = bf16[2,512,2,32]{1,3,2,0:T(8,128)(2,1)S(1)} fusion(bf16[2,512,2,32]{1,3,2,0:T(8,128)(2,1)S(1)} %copy-done.9, s32[]{:T(128)} %get-tuple-element.268, f32[2,512]{1,0:T(2,128)S(1)} %fusion.213, bf16[4096,32]{0,1:T(8,128)(2,1)S(1)} %get-tuple-element.278, bf16[4096,32]{0,1:T(8,128)(2,1)S(1)} %get-tuple-element.277, ...), kind=kOutput, calls=%fused_computation.28.clone.1 | convolution fusion | flops 553686016 | bytes 660480 | tf_op jit(solution)/shard_map/while/body/eval_jaxpr/hqk,kd->qhd/dot_general | solution.py:96
  64.0 6.7 %fusion.213 = f32[2,512]{1,0:T(2,128)S(1)} fusion(bf16[4096,32]{0,1:T(8,128)(2,1)S(1)} %get-tuple-element.277, bf16[2,512,2,32]{1,3,2,0:T(8,128)(2,1)} %get-tuple-element.276, s32[]{:T(128)} %get-tuple-element.268), kind=kOutput, calls=%fused_computation.190.clone.1 | convolution fusion | flops 281022464 | bytes 332288 | tf_op jit(solution)/shard_map/while/body/eval_jaxpr/sub | solution.py:94
  70.6 6.0 %fusion.214 = bf16[2,512,2,32]{1,3,2,0:T(8,128)(2,1)S(1)} fusion(bf16[2,512,2,32]{1,3,2,0:T(8,128)(2,1)S(1)} %copy-done.9, s32[]{:T(128)} %get-tuple-element.268, f32[2,512]{1,0:T(2,128)S(1)} %fusion.213, bf16[4096,32]{0,1:T(8,128)(2,1)S(1)} %get-tuple-element.278, bf16[4096,32]{0,1:T(8,128)(2,1)S(1)} %get-tuple-element.277, ...), kind=kOutput, calls=%fused_computation.28.clone.1 | convolution fusion | flops 553686016 | bytes 660480 | tf_op jit(solution)/shard_map/while/body/eval_jaxpr/hqk,kd->qhd/dot_general | solution.py:96
  79.6 10.2 %all-to-all-start.1 = ((bf16[16,2,2048]{2,1,0:T(2,128)(2,1)}), bf16[16,2,2048]{2,1,0:T(2,128)(2,1)S(1)}, u32[]{:S(2)}, u32[]{:S(2)}) async-start(bf16[16,2,2048]{2,1,0:T(2,128)(2,1)} %reshape.640), calls=%async_computation.1 | async-start | bytes 262144 | tf_op jit(solution)/shard_map/all_to_all | solution.py:175
  90.7 1.5 copy.119
  92.2 1.4 copy.120
  93.6 11.9 %while.20 = (s32[]{:T(128)}, bf16[2,512,1,64]{1,3,2,0:T(8,128)(2,1)}, bf16[2,512,1,64]{1,3,2,0:T(8,128)(2,1)S(1)}, bf16[4096,64]{1,0:T(8,128)(2,1)S(1)}, bf16[4096,64]{1,0:T(8,128)(2,1)}, /*index=5*/s32[]{:T(128)}) while((s32[]{:T(128)}, bf16[2,512,1,64]{1,3,2,0:T(8,128)(2,1)}, bf16[2,512,1,64]{1,3,2,0:T(8,128)(2,1)S(1)}, ...), condition=%wide.region_6.7_spmd, body=%wide.region_3.6_spmd.sunk | while | flops 555777024 | bytes 28977764 | solution.py:100
  93.6 1.4 multiply_reduce_fusion.4
  95.0 1.5 fusion.205
  96.5 3.1 %fusion.206 = bf16[2,512,1,64]{1,3,2,0:T(8,128)(2,1)} fusion(bf16[2,512,1,64]{1,3,2,0:T(8,128)(2,1)} %get-tuple-element.251, s32[]{:T(128)} %get-tuple-element.250, bf16[4096,64]{1,0:T(8,128)(2,1)S(1)} %copy-done.3, f32[512]{0:T(512)S(1)} %fusion.205, f32[512]{0:T(512)S(1)} %get-tuple-element.238, f32[512,4096]{1,0:T(8,128)S(1)} %get-tuple-element.237), kind=kOutput, calls=%fused_computation.10.clone.1 | convolution fusion | flops 276856832 | bytes 8983040 | tf_op jit(solution)/shard_map/while/body/eval_jaxpr/hqk,kd->qhd/dot_general | solution.py:96
  99.6 1.4 multiply_reduce_fusion.4
  101.0 1.5 fusion.205
  102.5 3.1 %fusion.206 = bf16[2,512,1,64]{1,3,2,0:T(8,128)(2,1)} fusion(bf16[2,512,1,64]{1,3,2,0:T(8,128)(2,1)} %get-tuple-element.251, s32[]{:T(128)} %get-tuple-element.250, bf16[4096,64]{1,0:T(8,128)(2,1)S(1)} %copy-done.3, f32[512]{0:T(512)S(1)} %fusion.205, f32[512]{0:T(512)S(1)} %get-tuple-element.238, f32[512,4096]{1,0:T(8,128)S(1)} %get-tuple-element.237), kind=kOutput, calls=%fused_computation.10.clone.1 | convolution fusion | flops 276856832 | bytes 8983040 | tf_op jit(solution)/shard_map/while/body/eval_jaxpr/hqk,kd->qhd/dot_general | solution.py:96
  107.9 7.2 %all-to-all-start = ((bf16[16,2,2048]{2,1,0:T(2,128)(2,1)}), bf16[16,2,2048]{2,1,0:T(2,128)(2,1)S(1)}, u32[]{:S(2)}, u32[]{:S(2)}) async-start(bf16[16,2,2048]{2,1,0:T(2,128)(2,1)} %reshape.638), calls=%async_computation | async-start | bytes 262144 | tf_op jit(solution)/shard_map/all_to_all | solution.py:174
  116.1 7.9 %all-to-all-done = bf16[16,2,2048]{2,1,0:T(2,128)(2,1)S(1)} async-done(((bf16[16,2,2048]{2,1,0:T(2,128)(2,1)}), bf16[16,2,2048]{2,1,0:T(2,128)(2,1)S(1)}, u32[]{:S(2)}, u32[]{:S(2)}) %all-to-all-start) | async-done | bytes 131104 | tf_op jit(solution)/shard_map/all_to_all | solution.py:174
  124.2 3.1 %fusion.174 = f32[64,2048]{1,0:T(8,128)S(1)} fusion(bf16[64,1024]{0,1:T(8,128)(2,1)S(1)} %bitcast.213, bf16[1024,2048]{1,0:T(8,128)(2,1)} %all-gather.3.cloned.1.call-done), kind=kOutput, calls=%fused_computation.197 | convolution fusion | flops 268435456 | bytes 4849664 | tf_op jit(solution)/shard_map/dot_general | solution.py:177
  127.4 3.3 %fusion.172 = (f32[64]{0:T(128)S(1)}, f32[64,2048]{1,0:T(8,128)S(1)}) fusion(f32[64,2048]{1,0:T(8,128)S(1)} %fusion.174, bf16[64,1024]{0,1:T(8,128)(2,1)S(1)} %bitcast.212, bf16[1024,2048]{1,0:T(8,128)(2,1)} %all-gather.5.cloned.1.call-done, bf16[64,2048]{1,0:T(8,128)(2,1)S(1)} %copy-done.8), kind=kOutput, calls=%fused_computation.193 | convolution fusion | flops 269090752 | bytes 5636352 | tf_op jit(solution)/shard_map/dot_general | solution.py:182
  131.0 1.4 convolution_convert_fusion.outgoing
  132.8 139.0 %shard_map.253 = f32[64,2048]{1,0:T(8,128)} custom-call(bf16[256,2048]{1,0:T(8,128)(2,1)} %convolution_convert_fusion.outgoing, f32[64,256]{1,0:T(8,128)} %get-tuple-element.106.mixing, bf16[80,128]{1,0:T(8,128)(2,1)} %constant.196.clone.pack, bf16[128,80]{1,0:T(8,128)(2,1)} %constant.197.clone.spread, bf16[2,2048,192]{2,1,0:T(8,128)(2,1)} %copy.130.gate_hbm, ...), custom_call_target="tpu_custom_call" | custom-call | flops 6000000000 | bytes 10000000 | tf_op jit(solution)/shard_map/pallas_call | solution.py:561
  271.9 1.9 fusion.173
  (124 shorter events, 28.6 us)
Async XLA Ops:
  6.5 265.3 %copy-start = (bf16[256,2048]{1,0:T(8,128)(2,1)S(1)}, bf16[256,2048]{1,0:T(8,128)(2,1)}, u32[]{:S(2)}) copy-start(bf16[256,2048]{1,0:T(8,128)(2,1)} %param.53) | copy-start | bytes 3145732
  6.5 117.7 %all-gather.3.cloned.1.call-start = ((), (), s32[]{:S(2)}) async-start(), calls=%async_computation.2 | async-start | bytes 4456448 | tf_op jit(solution)/shard_map/all_gather | solution.py:179
  7.3 120.1 %all-gather.5.cloned.1.call-start = ((), (), s32[]{:S(2)}) async-start(), calls=%async_computation.3 | async-start | bytes 4456448 | tf_op jit(solution)/shard_map/all_gather | solution.py:184
  10.1 30.0 %copy-start.16 = (s32[64,2]{0,1:T(2,128)S(1)}, s32[64,2]{0,1:T(2,128)}, u32[]{:S(2)}) copy-start(s32[64,2]{0,1:T(2,128)} %param.46) | copy-start | bytes 1540
  10.2 31.3 %copy-start.1 = (bf16[2,2048,192]{1,2,0:T(8,128)(2,1)S(1)}, bf16[2,2048,192]{1,2,0:T(8,128)(2,1)}, u32[]{:S(2)}) copy-start(bf16[2,2048,192]{1,2,0:T(8,128)(2,1)} %param.48) | copy-start | bytes 4718596
  10.4 10.5 %copy-start.6 = (bf16[1024,32]{0,1:T(8,128)(2,1)}, bf16[1024,32]{0,1:T(8,128)(2,1)S(1)}, u32[]{:S(2)}) copy-start(bf16[1024,32]{0,1:T(8,128)(2,1)S(1)} %copy.137) | copy-start | bytes 196612
  11.7 9.2 %copy-start.7 = (bf16[1024,32]{0,1:T(8,128)(2,1)}, bf16[1024,32]{0,1:T(8,128)(2,1)S(1)}, u32[]{:S(2)}) copy-start(bf16[1024,32]{0,1:T(8,128)(2,1)S(1)} %maximum_bitcast_fusion.1) | copy-start | bytes 196612
  15.7 5.2 %copy-start.2 = (bf16[1024,64]{0,1:T(8,128)(2,1)}, bf16[1024,64]{0,1:T(8,128)(2,1)S(1)}, u32[]{:S(2)}) copy-start(bf16[1024,64]{0,1:T(8,128)(2,1)S(1)} %maximum_bitcast_fusion) | copy-start | bytes 393220
  15.8 9.7 %collective-permute-start = (bf16[1024,192]{0,1:T(8,128)(2,1)S(1)}, bf16[1024,192]{0,1:T(8,128)(2,1)}, u32[]{:S(2)}, u32[]{:S(2)}) collective-permute-start(bf16[1024,192]{0,1:T(8,128)(2,1)S(1)} %pad_maximum_fusion), channel_id=1, source_target_pairs={{0,16},{16,0},{32,48},{48,32},{64,80},{80,64},{96,112},{112,96},{1... | collective-permute-start | bytes 1179656 | tf_op jit(solution)/shard_map/ppermute | solution.py:27
  27.1 21.4 %collective-permute-start.1 = (bf16[2048,192]{0,1:T(8,128)(2,1)S(1)}, bf16[2048,192]{0,1:T(8,128)(2,1)}, u32[]{:S(2)}, u32[]{:S(2)}) collective-permute-start(bf16[2048,192]{0,1:T(8,128)(2,1)S(1)} %maximum_select_fusion.1), channel_id=1, source_target_pairs={{0,32},{16,48},{32,0},{48,16},{64,96},{80,112},{96,64},{112,80},{1... | collective-permute-start | bytes 2359304 | tf_op jit(solution)/shard_map/ppermute | solution.py:27
  50.6 6.7 %copy-start.9 = (bf16[2,512,2,32]{1,3,2,0:T(8,128)(2,1)S(1)}, bf16[2,512,2,32]{1,3,2,0:T(8,128)(2,1)}, u32[]{:S(2)}) copy-start(bf16[2,512,2,32]{1,3,2,0:T(8,128)(2,1)} %get-tuple-element.269) | copy-start | bytes 393220 | tf_op jit(solution)/shard_map/while
  50.6 6.7 %copy-start.11 = (bf16[2,512,2,32]{1,3,2,0:T(8,128)(2,1)S(1)}, bf16[2,512,2,32]{1,3,2,0:T(8,128)(2,1)}, u32[]{:S(2)}) copy-start(bf16[2,512,2,32]{1,3,2,0:T(8,128)(2,1)} %get-tuple-element.276) | copy-start | bytes 393220 | tf_op jit(solution)/shard_map/while
  63.3 0.7 copy-start.10
  64.0 6.7 %copy-start.9 = (bf16[2,512,2,32]{1,3,2,0:T(8,128)(2,1)S(1)}, bf16[2,512,2,32]{1,3,2,0:T(8,128)(2,1)}, u32[]{:S(2)}) copy-start(bf16[2,512,2,32]{1,3,2,0:T(8,128)(2,1)} %get-tuple-element.269) | copy-start | bytes 393220 | tf_op jit(solution)/shard_map/while
  64.0 6.7 %copy-start.11 = (bf16[2,512,2,32]{1,3,2,0:T(8,128)(2,1)S(1)}, bf16[2,512,2,32]{1,3,2,0:T(8,128)(2,1)}, u32[]{:S(2)}) copy-start(bf16[2,512,2,32]{1,3,2,0:T(8,128)(2,1)} %get-tuple-element.276) | copy-start | bytes 393220 | tf_op jit(solution)/shard_map/while
  76.7 0.7 copy-start.10
  79.6 28.3 %all-to-all-start.1 = ((bf16[16,2,2048]{2,1,0:T(2,128)(2,1)}), bf16[16,2,2048]{2,1,0:T(2,128)(2,1)S(1)}, u32[]{:S(2)}, u32[]{:S(2)}) async-start(bf16[16,2,2048]{2,1,0:T(2,128)(2,1)} %reshape.640), calls=%async_computation.1 | async-start | bytes 262144 | tf_op jit(solution)/shard_map/all_to_all | solution.py:175
  93.6 21.5 %copy-start.17 = (s32[64,2]{0,1:T(2,128)S(1)}, s32[64,2]{0,1:T(2,128)}, u32[]{:S(2)}) copy-start(s32[64,2]{0,1:T(2,128)} %param.46) | copy-start | bytes 1540
  93.6 21.5 %copy-start.18 = (s32[64,2]{0,1:T(2,128)S(1)}, s32[64,2]{0,1:T(2,128)}, u32[]{:S(2)}) copy-start(s32[64,2]{0,1:T(2,128)} %copy.129) | copy-start | bytes 1540
  93.6 21.5 %copy-start.19 = (f32[64,2]{0,1:T(2,128)S(1)}, f32[64,2]{0,1:T(2,128)}, u32[]{:S(2)}) copy-start(f32[64,2]{0,1:T(2,128)} %param.47) | copy-start | bytes 1540
  95.0 1.5 copy-start.3
  101.0 1.5 copy-start.3
  105.6 21.8 %copy-start.8 = (bf16[64,2048]{1,0:T(8,128)(2,1)S(1)}, bf16[64,2048]{1,0:T(8,128)(2,1)}, u32[]{:S(2)}) copy-start(bf16[64,2048]{1,0:T(8,128)(2,1)} %param.31) | copy-start | bytes 786436
  107.9 16.1 %all-to-all-start = ((bf16[16,2,2048]{2,1,0:T(2,128)(2,1)}), bf16[16,2,2048]{2,1,0:T(2,128)(2,1)S(1)}, u32[]{:S(2)}, u32[]{:S(2)}) async-start(bf16[16,2,2048]{2,1,0:T(2,128)(2,1)} %reshape.638), calls=%async_computation | async-start | bytes 262144 | tf_op jit(solution)/shard_map/all_to_all | solution.py:174
  127.3 3.6 %copy-start.12 = (f32[2048]{0:T(1024)S(1)}, f32[2048]{0:T(1024)}, u32[]{:S(2)}) copy-start(f32[2048]{0:T(1024)} %param.45) | copy-start | bytes 24580
  127.3 3.6 %copy-start.13 = (f32[2048]{0:T(1024)S(1)}, f32[2048]{0:T(1024)}, u32[]{:S(2)}) copy-start(f32[2048]{0:T(1024)} %param.44) | copy-start | bytes 24580
  127.3 5.1 %copy-start.4 = (bf16[2048,256]{1,0:T(8,128)(2,1)S(1)}, bf16[2048,256]{1,0:T(8,128)(2,1)}, u32[]{:S(2)}) copy-start(bf16[2048,256]{1,0:T(8,128)(2,1)} %param.51) | copy-start | bytes 3145732
  132.8 139.1 %copy-start.5 = (bf16[2048,256]{1,0:T(8,128)(2,1)S(1)}, bf16[2048,256]{1,0:T(8,128)(2,1)}, u32[]{:S(2)}) copy-start(bf16[2048,256]{1,0:T(8,128)(2,1)} %param.52) | copy-start | bytes 3145732
  132.8 141.3 %copy-start.14 = (f32[2048]{0:T(1024)S(1)}, f32[2048]{0:T(1024)}, u32[]{:S(2)}) copy-start(f32[2048]{0:T(1024)} %param.55) | copy-start | bytes 24580
  132.8 141.3 %copy-start.15 = (f32[2048]{0:T(1024)S(1)}, f32[2048]{0:T(1024)}, u32[]{:S(2)}) copy-start(f32[2048]{0:T(1024)} %param.54) | copy-start | bytes 24580
Sparse Core Ops, SparseCore 0:
  9.2 46.2 all-gather.2
  57.2 41.3 all-gather.4

commit v2 on v1

--- a/solution.py
+++ b/solution.py
@@ -8,9 +8,7 @@
 from jax.experimental.pallas import tpu as pltpu
 from jax.sharding import PartitionSpec as P
 
-WIDE_HEADS = 16
 WIDE_GROUPS = 4
-NARROW_HEADS = 32
 NARROW_GROUPS = 8
 GRID_WIDTH = 64
 SEQ_SHARDS = 4
@@ -21,38 +19,6 @@
 EPS_LAYER = 1e-05
 ALPHA = 2.0**0.25
 THETA = 10000.0
-
-
-def swapped(x, axis, apart):
-    return lax.ppermute(x, axis, [(i, i ^ 1 << apart) for i in range(lax.axis_size(axis))])
-
-
-def head_norm(values, gain_vec):
-    mean_square = jnp.mean(values * values, axis=-1, keepdims=True)
-    return values * lax.rsqrt(mean_square + EPS_HEAD) * gain_vec
-
-
-def rotate(values, position):
-    half_size = values.shape[-1] // 2
-    frequency = THETA ** (-jnp.arange(half_size, dtype=jnp.float32) / half_size)
-    angles = position.astype(jnp.float32)[:, None] * frequency
-    cosine = jnp.cos(angles)[:, None, :]
-    sine_part = jnp.sin(angles)[:, None, :]
-    leading = values[..., :half_size]
-    trailing = values[..., half_size:]
-    return jnp.concatenate(
-        [leading * cosine - trailing * sine_part, trailing * cosine + leading * sine_part], axis=-1
-    )
-
-
-def grid_rotate(values, position):
-    half_size = values.shape[-1] // 2
-    grid_row = position // GRID_WIDTH
-    grid_col = position % GRID_WIDTH
-    return jnp.concatenate(
-        [rotate(values[..., :half_size], grid_row), rotate(values[..., half_size:], grid_col)],
-        axis=-1,
-    )
 
 
 def layer_norm(values, gain_vec, bias_vec):
@@ -60,45 +26,6 @@
     shifted = values - center
     variance = jnp.mean(shifted * shifted, axis=-1, keepdims=True)
     return (shifted * lax.rsqrt(variance + EPS_LAYER) * gain_vec + bias_vec).astype(jnp.bfloat16)
-
-
-def prepare(queries, key_block, value_block, query_gain, key_gain, heads_total, groups, position):
-    head_size = query_gain.shape[0]
-    local_heads = queries.shape[1] // head_size
-    group_index = lax.axis_index("tp") * local_heads // (heads_total // groups)
-    query_rows = queries.reshape(queries.shape[0], local_heads, head_size).astype(jnp.float32)
-    rotated_queries = grid_rotate(head_norm(query_rows, query_gain), position).astype(jnp.bfloat16)
-    column_start = group_index * head_size
-    key_rows = lax.dynamic_slice_in_dim(key_block, column_start, head_size, 1).astype(jnp.float32)[
-        :, None, :
-    ]
-    rotated_keys = grid_rotate(head_norm(key_rows, key_gain), position)[:, 0, :].astype(
-        jnp.bfloat16
-    )
-    value_rows = lax.dynamic_slice_in_dim(value_block, column_start, head_size, 1)
-    return (rotated_queries, jnp.concatenate([rotated_keys, value_rows], axis=1))
-
-
-def attend_local(rotated_queries, key_block, value_block):
-    seg_rows, local_heads, head_size = rotated_queries.shape
-    block_rows = min(512, seg_rows)
-    score_scale = head_size ** (-0.5)
-    blocks = rotated_queries.reshape(seg_rows // block_rows, block_rows, local_heads, head_size)
-
-    def one_block(query_block):
-        scores = (
-            jnp.einsum("qhd,kd->hqk", query_block, key_block, preferred_element_type=jnp.float32)
-            * score_scale
-        )
-        largest = jnp.max(scores, axis=-1, keepdims=True)
-        weights = jnp.exp(scores - largest)
-        weights = (weights / jnp.sum(weights, axis=-1, keepdims=True)).astype(jnp.bfloat16)
-        return jnp.einsum(
-            "hqk,kd->qhd", weights, value_block, preferred_element_type=jnp.float32
-        ).astype(jnp.bfloat16)
-
-    mixed_rows = lax.map(one_block, blocks)
-    return mixed_rows.reshape(seg_rows, local_heads * head_size)
 
 
 def local(
@@ -128,61 +55,20 @@
     second_gain,
     second_bias,
 ):
-    seg_rows = wide_query.shape[0]
-    position = lax.axis_index("sp") % SEQ_SHARDS * seg_rows + jnp.arange(seg_rows, dtype=jnp.int32)
-    wide_rotated, wide_pack = prepare(
+    projected = attention(
         wide_query,
+        narrow_query,
         wide_keys,
+        narrow_keys,
         wide_values,
+        narrow_values,
         wide_query_gain,
         wide_key_gain,
-        WIDE_HEADS,
-        WIDE_GROUPS,
-        position,
-    )
-    narrow_rotated, narrow_pack = prepare(
-        narrow_query,
-        narrow_keys,
-        narrow_values,
         narrow_query_gain,
         narrow_key_gain,
-        NARROW_HEADS,
-        NARROW_GROUPS,
-        position,
-    )
-    gathered = jnp.concatenate([wide_pack, narrow_pack], axis=1)
-    for level in range(SEQ_SHARDS.bit_length() - 1):
-        partner = swapped(gathered, "sp", level)
-        is_upper = lax.axis_index("sp") // 2**level % 2 == 1
-        gathered = jnp.where(
-            is_upper,
-            jnp.concatenate([partner, gathered], axis=0),
-            jnp.concatenate([gathered, partner], axis=0),
-        )
-    wide_size = wide_query_gain.shape[0]
-    narrow_size = narrow_query_gain.shape[0]
-    narrow_start = 2 * wide_size
-    wide_mixed = attend_local(
-        wide_rotated, gathered[:, :wide_size], gathered[:, wide_size:narrow_start]
-    )
-    narrow_mixed = attend_local(
-        narrow_rotated,
-        gathered[:, narrow_start : narrow_start + narrow_size],
-        gathered[:, narrow_start + narrow_size :],
-    )
-    wide_tokens, narrow_tokens = (
-        lax.all_to_all(wide_mixed, "tp", split_axis=0, concat_axis=1, tiled=True),
-        lax.all_to_all(narrow_mixed, "tp", split_axis=0, concat_axis=1, tiled=True),
-    )
-    running = jnp.dot(
-        wide_tokens,
-        lax.all_gather(wide_out, "tp", axis=0, tiled=True),
-        preferred_element_type=jnp.float32,
-    )
-    projected = running + jnp.dot(
-        narrow_tokens,
-        lax.all_gather(narrow_out, "tp", axis=0, tiled=True),
-        preferred_element_type=jnp.float32,
+        wide_out,
+        narrow_out,
+        lax.axis_size("tp") // 2,
     )
     hidden = layer_norm(ALPHA * residual.astype(jnp.float32) + projected, first_gain, first_bias)
     device_rows = hidden.shape[0]
@@ -225,6 +111,12 @@
 CAPACITY = 5
 SLOT = 8
 MESH = pl.DeviceIdType.MESH
+
+
+def dot_rows(a, b):
+    return lax.dot_general(
+        a, b, (((1,), (1,)), ((), ())), preferred_element_type=jnp.float32
+    )
 
 
 def moe_kernel(
@@ -418,8 +310,8 @@
         rows = blocks[block].reshape(-1, blocks.shape[-1])
         total = None
         for side in range(2):
-            gate_values = jnp.dot(rows, gate_w[side], preferred_element_type=jnp.float32)
-            up_values = jnp.dot(rows, up_w[side], preferred_element_type=jnp.float32)
+            gate_values = dot_rows(rows, gate_w[side])
+            up_values = dot_rows(rows, up_w[side])
             active = (gate_values / (1.0 + jnp.exp(-gate_values)) * up_values).astype(
                 jnp.bfloat16
             )
@@ -570,8 +462,8 @@
             pltpu.VMEM((2, half, 2, half_rows, width), bf16),
             pltpu.VMEM((2, n_sp * SLOT, width), bf16),
             pltpu.VMEM((2 * n_sp * SLOT, width), bf16),
-            pltpu.VMEM((2, width, hidden_units), bf16),
-            pltpu.VMEM((2, width, hidden_units), bf16),
+            pltpu.VMEM((2, hidden_units, width), bf16),
+            pltpu.VMEM((2, hidden_units, width), bf16),
             pltpu.VMEM((2, hidden_units, width), bf16),
             dma((2 * n_sp,)),
             dma((2 * n_sp,)),
@@ -596,9 +488,558 @@
         mixing,
         jnp.asarray(pack, bf16),
         jnp.asarray(pack.T, bf16),
-        expert_gate,
-        expert_up,
+        jnp.swapaxes(expert_gate, 1, 2),
+        jnp.swapaxes(expert_up, 1, 2),
         expert_down,
+    )
+
+
+LANES = 256
+LOG2E = 1.4426950408889634
+
+
+def iota2(shape, axis):
+    return lax.broadcasted_iota(jnp.int32, shape, axis)
+
+
+def selection(rows, column_of_lane, offset, first, last):
+    lane = iota2((rows, LANES), 1)
+    row = iota2((rows, LANES), 0)
+    inside = jnp.logical_and(lane >= first, lane < last)
+    hit = jnp.logical_and(inside, row == column_of_lane(lane - first) + offset)
+    return jnp.where(hit, 1.0, 0.0).astype(jnp.bfloat16)
+
+
+def flip(apart):
+    return lambda lane: lane + apart - 2 * apart * ((lane // apart) % 2)
+
+
+def same(lane):
+    return lane
+
+
+def bf16_dot(a, b):
+    return jnp.dot(a, b, preferred_element_type=jnp.float32)
+
+
+def turned_dot(a, b):
+    return lax.dot_general(
+        a, b, (((0,), (0,)), ((), ())), preferred_element_type=jnp.float32
+    )
+
+
+def turned(raw, swapped_raw, mean_matrix, row_tables, tables, gains, first_row, rows):
+    square = raw * raw
+    high = square.astype(jnp.bfloat16)
+    low = (square - high.astype(jnp.float32)).astype(jnp.bfloat16)
+    mean_square = bf16_dot(high, mean_matrix) + bf16_dot(low, mean_matrix)
+    shape = (rows * GRID_WIDTH, LANES)
+    cosine = (row_tables[0, pl.ds(first_row, rows)] + tables[0][None]).reshape(shape)
+    sine = (row_tables[1, pl.ds(first_row, rows)] + tables[1][None]).reshape(shape)
+    mixed = raw * (cosine * gains[0:1]) + swapped_raw * (sine * gains[1:2])
+    return mixed * lax.rsqrt(mean_square + EPS_HEAD)
+
+
+def attention_kernel(
+    n_z,
+    wide_query,
+    narrow_query,
+    wide_keys,
+    narrow_keys,
+    wide_values,
+    narrow_values,
+    gains,
+    row_tables,
+    tables,
+    out_rows,
+    projected,
+    own_kv,
+    kv,
+    queries,
+    totals,
+    largest,
+    mixed,
+    mixed_in,
+    sums,
+    landing,
+    weights,
+    final_out,
+    final_in,
+    kv_send,
+    kv_recv,
+    far_send,
+    far_recv,
+    pass_send,
+    pass_recv,
+    mixed_send,
+    mixed_recv,
+    sum_send,
+    sum_recv,
+    weight_sem,
+    weight_send,
+    weight_recv,
+    final_send,
+    final_recv,
+):
+    half = n_z // 2
+    sp = lax.axis_index("sp")
+    tp = lax.axis_index("tp")
+    z = tp // 2
+    core = tp % 2
+    x = sp % SEQ_SHARDS
+    row_start = sp - x
+    right = (sp, 2 * ((z + 1) % n_z) + core)
+    left = (sp, 2 * ((z + n_z - 1) % n_z) + core)
+    east = (row_start + (x + 1) % SEQ_SHARDS, tp)
+    west = (row_start + (x + SEQ_SHARDS - 1) % SEQ_SHARDS, tp)
+    partner = (sp, 2 * z + 1 - core)
+    quarter = kv.shape[2]
+    columns = weights.shape[2]
+    chip_rows = queries.shape[2]
+    core_rows = chip_rows // 2
+
+    def remote(src, dst, send_sem, recv_sem, device):
+        return pltpu.make_async_remote_copy(
+            src_ref=src,
+            dst_ref=dst,
+            send_sem=send_sem,
+            recv_sem=recv_sem,
+            device_id=device,
+            device_id_type=MESH,
+        )
+
+    def column_half(which):
+        return out_rows.at[:, pl.ds(pl.multiple_of(which * columns, columns), columns)]
+
+    own_weights = pltpu.make_async_copy(column_half(core), weights.at[0], weight_sem)
+    own_weights.start()
+    barrier = pltpu.get_barrier_semaphore()
+    for device in (right, left, east, west, partner):
+        pl.semaphore_signal(barrier, inc=1, device_id=device, device_id_type=MESH)
+
+    wide_group = tp * WIDE_GROUPS // (2 * n_z)
+    narrow_group = tp * NARROW_GROUPS // (2 * n_z)
+    lane_in = iota2((LANES, LANES), 0)
+    lane_out = iota2((LANES, LANES), 1)
+    both_wide = jnp.logical_and(lane_in < 64, lane_out < 64)
+    both_narrow = jnp.logical_and(
+        jnp.logical_and(lane_in >= 128, lane_in < 160),
+        jnp.logical_and(lane_out >= 128, lane_out < 160),
+    )
+    mean_matrix = jnp.where(both_wide, 1.0 / 64, jnp.where(both_narrow, 1.0 / 32, 0.0)).astype(
+        jnp.bfloat16
+    )
+    key_in = wide_keys.shape[1]
+    wide_same = selection(key_in, same, 64 * wide_group, 0, 64)
+    wide_flip = selection(key_in, flip(16), 64 * wide_group, 0, 64)
+    narrow_same = selection(key_in, same, 32 * narrow_group, 128, 160)
+    narrow_flip = selection(key_in, flip(8), 32 * narrow_group, 128, 160)
+    wide_place = selection(key_in, same, 64 * wide_group, 64, 128)
+    narrow_place = selection(key_in, same, 32 * narrow_group, 160, 192) + selection(
+        key_in, same, 32 * narrow_group, 224, 256
+    )
+    lane = iota2((1, LANES), 1)
+    ones = jnp.where(jnp.logical_and(lane >= 192, lane < 224), 1.0, 0.0)
+    grid_rows = quarter // GRID_WIDTH
+    first_row = x * (SEQ_SHARDS * grid_rows)
+
+    def kv_copy(to_east):
+        return remote(
+            own_kv.at[pl.ds(2 * core, 2)],
+            kv.at[x, pl.ds(2 * core, 2)],
+            kv_send.at[to_east],
+            kv_recv.at[to_east],
+            west if to_east == 0 else east,
+        )
+
+    def kv_arrival(to_east):
+        source = (x + (SEQ_SHARDS - 1 if to_east == 1 else 1)) % SEQ_SHARDS
+        return source, remote(
+            own_kv.at[pl.ds(2 * core, 2)],
+            kv.at[source, pl.ds(2 * core, 2)],
+            kv_send.at[to_east],
+            kv_recv.at[to_east],
+            west if to_east == 0 else east,
+        )
+
+    def far_copy(to_east, arriving):
+        source = (x + (SEQ_SHARDS - 1 if to_east == 1 else 1)) % SEQ_SHARDS
+        block = (x + 2) % SEQ_SHARDS if arriving else source
+        part = 2 * core + (0 if to_east == 1 else 1)
+        return remote(
+            kv.at[block, part],
+            kv.at[block, part],
+            far_send.at[to_east],
+            far_recv.at[to_east],
+            west if to_east == 0 else east,
+        )
+
+    def pass_copy(to_east, side):
+        source = (x + (SEQ_SHARDS - 1 if to_east == 1 else 1)) % SEQ_SHARDS
+        at = pl.ds(2 * side, 2)
+        return remote(
+            kv.at[source, at],
+            kv.at[source, at],
+            pass_send.at[to_east],
+            pass_recv.at[to_east],
+            partner,
+        )
+
+    def pass_far(to_east, side):
+        block = (x + 2) % SEQ_SHARDS
+        part = 2 * side + (0 if to_east == 1 else 1)
+        return remote(
+            kv.at[block, part],
+            kv.at[block, part],
+            pass_send.at[2 + to_east],
+            pass_recv.at[2 + to_east],
+            partner,
+        )
+
+    def prepare_keys(i, carry):
+        part = (2 * core + i) % 4
+        at = pl.ds(pl.multiple_of(part * quarter, quarter), quarter)
+        wide = wide_keys[at, :]
+        narrow = narrow_keys[at, :]
+        raw = bf16_dot(wide, wide_same) + bf16_dot(narrow, narrow_same)
+        other = bf16_dot(wide, wide_flip) + bf16_dot(narrow, narrow_flip)
+        keys = turned(
+            raw,
+            other,
+            mean_matrix,
+            row_tables,
+            tables,
+            gains[0:2],
+            first_row + part * grid_rows,
+            grid_rows,
+        )
+        values = bf16_dot(wide_values[at, :], wide_place) + bf16_dot(
+            narrow_values[at, :], narrow_place
+        )
+        own_kv[part] = (keys + values + ones).astype(jnp.bfloat16)
+        return carry
+
+    lax.fori_loop(0, 2, prepare_keys, 0)
+    pl.semaphore_wait(barrier, 5)
+    for to_east in range(2):
+        kv_copy(to_east).start()
+    partner_weights = remote(
+        column_half(1 - core), weights.at[1], weight_send, weight_recv, partner
+    )
+    partner_weights.start()
+    lax.fori_loop(2, 4, prepare_keys, 0)
+
+    scales = (64**-0.5 * LOG2E, 32**-0.5 * LOG2E, 32**-0.5 * LOG2E)
+
+    def attend(chunk, keys, start):
+        for head in range(3):
+            scores = lax.dot_general(
+                queries[chunk, head],
+                keys,
+                (((1,), (1,)), ((), ())),
+                preferred_element_type=jnp.float32,
+            )
+            peak = jnp.max(scores, axis=-1, keepdims=True)
+            if not start:
+                before = largest[chunk, head][:, 0:1]
+                peak = jnp.maximum(before, peak)
+            parts = jnp.exp2((scores - peak) * scales[head]).astype(jnp.bfloat16)
+            fresh = bf16_dot(parts, keys)
+            if not start:
+                fresh = fresh + totals[chunk, head] * jnp.exp2((before - peak) * scales[head])
+            totals[chunk, head] = fresh
+            largest[chunk, head] = jnp.broadcast_to(peak, (chip_rows, 128))
+
+    def chunk_of(i):
+        hop = half - (i + 1) // 2
+        return (z + jnp.where(i % 2 == 1, hop, n_z - hop)) % n_z
+
+    query_in = wide_query.shape[0]
+    query_same = (
+        selection(query_in, same, 0, 0, 64),
+        selection(query_in, same, 0, 128, 160),
+        selection(query_in, same, 32, 128, 160),
+    )
+    query_flip = (
+        selection(query_in, flip(16), 0, 0, 64),
+        selection(query_in, flip(8), 0, 128, 160),
+        selection(query_in, flip(8), 32, 128, 160),
+    )
+
+    def own_step(i, carry):
+        chunk = chunk_of(i)
+        at = pl.ds(pl.multiple_of(chunk * chip_rows, chip_rows), chip_rows)
+        chunk_grid = chip_rows // GRID_WIDTH
+        for head in range(3):
+            rows = (wide_query if head == 0 else narrow_query)[:, at]
+            queries[chunk, head] = turned(
+                turned_dot(rows, query_same[head]),
+                turned_dot(rows, query_flip[head]),
+                mean_matrix,
+                row_tables,
+                tables,
+                gains[2:4],
+                first_row + chunk * chunk_grid,
+                chunk_grid,
+            ).astype(jnp.bfloat16)
+        attend(chunk, own_kv[...].reshape(-1, LANES), True)
+        return carry
+
+    lax.fori_loop(0, n_z, own_step, 0)
+
+    for to_east in range(2):
+        kv_arrival(to_east)[1].wait_recv()
+        far_copy(to_east, False).start()
+        pass_copy(to_east, core).start()
+    for to_east in range(2):
+        pass_copy(to_east, 1 - core).wait_recv()
+
+    def next_block(i, b, carry):
+        block = (x + 3 - 2 * b + 3 * (b * (b - 1) // 2)) % SEQ_SHARDS
+        attend(chunk_of(i), kv[block].reshape(-1, LANES), False)
+        return carry
+
+    def near_step(j, carry):
+        return next_block(half + j // 2, j % 2, carry)
+
+    lax.fori_loop(0, 2 * (n_z - half), near_step, 0)
+
+    for to_east in range(2):
+        far_copy(to_east, True).wait_recv()
+        pass_far(to_east, core).start()
+    for to_east in range(2):
+        pass_far(to_east, 1 - core).wait_recv()
+    own_weights.wait()
+    partner_weights.wait()
+
+    def mixed_copy(i):
+        return remote(
+            mixed.at[i], mixed_in.at[i], mixed_send.at[i], mixed_recv.at[i], partner
+        )
+
+    def sum_copy(direction, step, h):
+        block = (
+            z + (half + 1 - step if direction == 0 else n_z - half - 1 + step)
+        ) % n_z
+        return block, remote(
+            sums.at[block, h],
+            landing.at[direction, step - 1, h],
+            sum_send.at[direction, step - 1, h],
+            sum_recv.at[direction, step - 1, h],
+            right if direction == 0 else left,
+        )
+
+    def add_and_send(direction, step, h):
+        block, copy = sum_copy(direction, step, h)
+        sum_copy(direction, step - 1, h)[1].wait_recv()
+        sums[block, h] = (
+            sums[block, h].astype(jnp.float32) + landing[direction, step - 2, h].astype(jnp.float32)
+        ).astype(jnp.bfloat16)
+        copy.start()
+
+    def step_body(i, carry):
+        @pl.when(i < n_z)
+        def _():
+            lax.fori_loop(
+                jnp.where(i < half, 0, 2), 3, functools.partial(next_block, i), 0
+            )
+            chunk = chunk_of(i)
+            joined = None
+            for head, (first, last) in enumerate(((64, 128), (160, 192), (224, 256))):
+                part = totals[chunk, head]
+                part = part / part[:, 192:193]
+                inside = jnp.logical_and(lane >= first, lane < last)
+                part = jnp.where(inside, part, 0.0)
+                joined = part if joined is None else joined + part
+            mixed[i] = joined.astype(jnp.bfloat16)
+            mixed_copy(i).start()
+
+        @pl.when(i >= 1)
+        def _():
+            j = i - 1
+            chunk = chunk_of(j)
+            mixed_copy(j).wait_recv()
+            total = bf16_dot(mixed[j], weights[0]) + bf16_dot(mixed_in[j], weights[1])
+            sums[chunk] = total.astype(jnp.bfloat16).reshape(sums.shape[1:])
+
+            @pl.when(j == 0)
+            def _():
+                for direction in range(2):
+                    sum_copy(direction, 1, 1 - direction)[1].start()
+
+            if half > 1:
+
+                @pl.when(j == 1)
+                def _():
+                    sum_copy(0, 2, 0)[1].start()
+
+                @pl.when(j == 2)
+                def _():
+                    sum_copy(1, 2, 1)[1].start()
+
+        @pl.when(jnp.logical_and(i >= 3, i <= n_z))
+        def _():
+            step = (i - 1) // 2 + 1
+            for direction in range(2):
+
+                @pl.when((i - 1) % 2 == direction)
+                def _(direction=direction):
+                    add_and_send(direction, step, 1 - direction)
+
+                    @pl.when(step > 2)
+                    def _():
+                        add_and_send(direction, step, direction)
+
+        return carry
+
+    lax.fori_loop(0, n_z + 1, step_body, 0)
+
+    for h in range(2):
+        total = sums[z, h].astype(jnp.float32)
+        for direction in range(2):
+            if h != direction or half > 1:
+                sum_copy(direction, half, h)[1].wait_recv()
+                total = total + landing[direction, half - 1, h].astype(jnp.float32)
+        final_out[h] = total
+
+    final_copy = remote(final_out.at[1 - core], final_in, final_send, final_recv, partner)
+    final_copy.start()
+
+    for to_east in range(2):
+        kv_copy(to_east).wait_send()
+        far_copy(to_east, False).wait_send()
+        pass_copy(to_east, core).wait_send()
+        pass_far(to_east, core).wait_send()
+    for direction in range(2):
+        for hop in range(1, half + 1):
+            for h in range(2):
+                if hop > 1 or h != direction:
+                    sum_copy(direction, hop, h)[1].wait_send()
+
+    def mixed_done(i, carry):
+        mixed_copy(i).wait_send()
+        return carry
+
+    lax.fori_loop(0, n_z, mixed_done, 0)
+    final_copy.wait()
+    for which in range(2):
+
+        @pl.when(core == which)
+        def _(which=which):
+            projected[:, which * columns : (which + 1) * columns] = final_out[which]
+            projected[:, (1 - which) * columns : (2 - which) * columns] = final_in[...]
+
+
+def turn_tables():
+    tables = np.zeros((4, GRID_WIDTH, LANES), np.float64)
+    for first, size in ((0, 64), (128, 32)):
+        n = size // 4
+        angle = np.arange(GRID_WIDTH)[:, None] * THETA ** (-np.arange(n)[None, :] / n)
+        cosine = np.concatenate([np.cos(angle)] * 2, axis=1)
+        sine = np.concatenate([-np.sin(angle), np.sin(angle)], axis=1)
+        tables[0, :, first : first + 2 * n] = cosine
+        tables[1, :, first : first + 2 * n] = sine
+        tables[2, :, first + 2 * n : first + 4 * n] = cosine
+        tables[3, :, first + 2 * n : first + 4 * n] = sine
+    tables = tables.astype(np.float32)
+    return tables[:2, :, None, :], tables[2:]
+
+
+def lane_gain(wide_gain, narrow_gain, flipped):
+    if flipped:
+        wide_gain = wide_gain.reshape(2, 2, 16)[:, ::-1].reshape(-1)
+        narrow_gain = narrow_gain.reshape(2, 2, 8)[:, ::-1].reshape(-1)
+    zeros = jnp.zeros((64,), jnp.float32)
+    return jnp.concatenate([wide_gain, zeros, narrow_gain, zeros, zeros[:32]])
+
+
+def attention(
+    wide_query,
+    narrow_query,
+    wide_keys,
+    narrow_keys,
+    wide_values,
+    narrow_values,
+    wide_query_gain,
+    wide_key_gain,
+    narrow_query_gain,
+    narrow_key_gain,
+    wide_out,
+    narrow_out,
+    n_z,
+):
+    rows = wide_query.shape[0]
+    chip_rows = rows // n_z
+    width = wide_out.shape[1]
+    half = n_z // 2
+    gains = jnp.stack(
+        [
+            lane_gain(wide_key_gain, narrow_key_gain, False),
+            lane_gain(wide_key_gain, narrow_key_gain, True),
+            lane_gain(wide_query_gain, narrow_query_gain, False),
+            lane_gain(wide_query_gain, narrow_query_gain, True),
+        ]
+    )
+    row_tables, tables = turn_tables()
+    gap = jnp.zeros((64, width), jnp.bfloat16)
+    out_rows = jnp.concatenate(
+        [gap, wide_out, gap[:32], narrow_out[:32], gap[:32], narrow_out[32:]], axis=0
+    )
+    vmem = pl.BlockSpec(memory_space=pltpu.VMEM)
+    dma = pltpu.SemaphoreType.DMA
+    bf16 = jnp.bfloat16
+    f32 = jnp.float32
+    return pl.pallas_call(
+        functools.partial(attention_kernel, n_z),
+        out_shape=jax.ShapeDtypeStruct((chip_rows // 2, width), f32),
+        in_specs=[vmem] * 10,
+        out_specs=vmem,
+        scratch_shapes=[
+            pltpu.VMEM((4, rows // 4, LANES), bf16),
+            pltpu.VMEM((SEQ_SHARDS, 4, rows // 4, LANES), bf16),
+            pltpu.VMEM((n_z, 3, chip_rows, LANES), bf16),
+            pltpu.VMEM((n_z, 3, chip_rows, LANES), f32),
+            pltpu.VMEM((n_z, 3, chip_rows, 128), f32),
+            pltpu.VMEM((n_z, chip_rows, LANES), bf16),
+            pltpu.VMEM((n_z, chip_rows, LANES), bf16),
+            pltpu.VMEM((n_z, 2, chip_rows // 2, width // 2), bf16),
+            pltpu.VMEM((2, half, 2, chip_rows // 2, width // 2), bf16),
+            pltpu.VMEM((2, LANES, width // 2), bf16),
+            pltpu.VMEM((2, chip_rows // 2, width // 2), f32),
+            pltpu.VMEM((chip_rows // 2, width // 2), f32),
+            dma((2,)),
+            dma((2,)),
+            dma((2,)),
+            dma((2,)),
+            dma((4,)),
+            dma((4,)),
+            dma((n_z,)),
+            dma((n_z,)),
+            dma((2, half, 2)),
+            dma((2, half, 2)),
+            dma,
+            dma,
+            dma,
+            dma,
+            dma,
+        ],
+        compiler_params=pltpu.CompilerParams(
+            collective_id=1, has_side_effects=True, vmem_limit_bytes=56 * 2**20
+        ),
+        cost_estimate=pl.CostEstimate(
+            flops=13_000_000_000, bytes_accessed=6_000_000, transcendentals=13_000_000
+        ),
+    )(
+        wide_query.T,
+        narrow_query.T,
+        wide_keys,
+        narrow_keys,
+        wide_values,
+        narrow_values,
+        gains,
+        jnp.asarray(row_tables),
+        jnp.asarray(tables),
+        out_rows,
     )
 
 

time: 283 us -> 247 us (0.87)
  Pallas kernels: 139 us -> 227 us
  matrix products: 44.3 us -> 3.71 us
  starting transfers between devices: 23.9 us -> 0 us
  local copies, waits for them, and re-layouts: 27.1 us -> 10.4 us
  other arithmetic: 20.1 us -> 5.6 us
  between operations: 14 us -> 0.26 us
  waiting for transfers between devices: 13.3 us -> 0 us
    pallas_call x0 -> x1, Pallas kernels: none -> 86.1 us  [attention(): pl.pallas_call(functools.partial(attention_kernel, n_z), out_shape=jax.Sh...]
    dot_general x8 -> x0, matrix products: 27.3 us -> none  [the longest x4 18.2 us: one_block(): jnp.einsum('hqk,kd->qhd', weights, value_block, preferred_element_type=jn...]
    all_to_all x2 -> x0, starting transfers between devices: 17.4 us -> none  [the longest x1 10.2 us: local(): lax.all_to_all(narrow_mixed, 'tp', split_axis=0, concat_axis=1, tiled=True)]
    sub x2 -> x0, matrix products: 13.3 us -> none  [one_block(): weights = jnp.exp(scores - largest)]
    all_to_all x2 -> x0, waiting for transfers between devices: 7.92 us -> none  [the longest x1 7.91 us: local(): lax.all_to_all(wide_mixed, 'tp', split_axis=0, concat_axis=1, tiled=True)]
    while x21 -> x0, local copies, waits for them, and re-layouts: 7.08 us -> none  [the longest x5 5.71 us: attend_local(): mixed_rows = lax.map(one_block, blocks)]
    ppermute x2 -> x0, starting transfers between devices: 6.45 us -> none  [swapped(): lax.ppermute(x, axis, [(i, i ^ 1 << apart) for i in range(lax.axis_size(a...]
    unnamed x43 -> x30, local copies, waits for them, and re-layouts: 9.05 us -> 3.96 us
  transfers between devices with their start and end apart: 6 -> 0, of which waited for: 2 -> 0; matrix products, arithmetic and copies ran while one was open for 29% -> 0% of each run, Pallas kernels for 0% -> 0%
where the time goes in v2:
time: 247 us
  Pallas kernels  227 us (92%)
  local copies, waits for them, and re-layouts  10.4 us (4%)
  other arithmetic  5.6 us (2%)
  matrix products  3.71 us (2%)
    pallas_call x1, Pallas kernels, moe(): pl.pallas_call(functools.partial(moe_kernel, n_sp, n_z), out_shape=jax.Sh...  141 us
    pallas_call x1, Pallas kernels, attention(): pl.pallas_call(functools.partial(attention_kernel, n_z), out_shape=jax.Sh...  86.1 us

profile of v2, /device:TPU:1, one launch (start us, length us, event | category | flops | bytes accessed | tf_op | source)
XLA Modules:
  0.0 246.7 jit_solution(11785926380553525113)
XLA Ops:
  0.0 0.8 reshape.72
  0.9 0.1 reshape.73
  0.9 0.7 reshape.74
  1.7 0.1 reshape.75
  1.9 0.7 reshape.76
  2.7 0.7 reshape.78
  3.5 0.1 reshape.79
  3.7 0.7 concatenate.15
  4.4 0.7 concatenate.17
  5.2 0.6 pad_maximum_fusion.gains
  5.8 1.0 constant_dynamic-update-slice_fusion
  6.8 0.9 slice_dynamic-update-slice_fusion.1
  7.7 0.9 slice_dynamic-update-slice_fusion.out_rows
  8.7 1.0 copy-done.5
  9.6 86.1 %shard_map.271 = f32[64,2048]{1,0:T(8,128)} custom-call(bf16[64,1024]{1,0:T(8,128)(2,1)} %bitcast.21, bf16[64,1024]{1,0:T(8,128)(2,1)} %bitcast.22, bf16[1024,256]{1,0:T(8,128)(2,1)} %wide_keys.1, bf16[1024,256]{1,0:T(8,128)(2,1)} %narrow_keys.1, bf16[1024,256]{1,0:T(8,128)(2,1)} %wide_values.1, bf16[1024,256]{1,0:T(8,128)(2,1)} %narrow_values.1, ...), custom_call_target="tpu_custom_call" | custom-call | flops 12999999488 | bytes 6000000 | tf_op jit(solution)/shard_map/pallas_call | solution.py:992
  95.8 1.3 fusion.1
  97.1 1.3 multiply_reduce_fusion.1
  98.4 0.2 add_convert_fusion.1
  98.6 0.1 copy.42
  98.7 0.1 eq.29
  98.8 0.1 fusion.7
  98.9 0.2 reduce_window_sum.11
  99.1 0.2 select_reduce_fusion.1
  99.2 0.1 reduce_sum.68
  99.5 0.7 select_reduce_fusion
  100.2 1.4 convolution_convert_fusion.outgoing
  101.7 140.7 %shard_map.272 = f32[64,2048]{1,0:T(8,128)} custom-call(bf16[256,2048]{1,0:T(8,128)(2,1)} %convolution_convert_fusion.outgoing, f32[64,256]{1,0:T(8,128)} %get-tuple-element.5.mixing, bf16[80,128]{1,0:T(8,128)(2,1)} %constant.39.clone.pack, bf16[128,80]{1,0:T(8,128)(2,1)} %constant.40.clone.spread, bf16[2,192,2048]{2,1,0:T(8,128)(2,1)} %bitcast.19, ...), custom_call_target="tpu_custom_call" | custom-call | flops 6000000000 | bytes 10000000 | tf_op jit(solution)/shard_map/pallas_call | solution.py:453
  242.4 0.3 fusion.12
  242.7 0.9 copy-done.4
  243.6 2.0 fusion.11
  245.6 0.2 multiply_reduce_fusion
  245.9 0.9 add_convert_fusion
  (40 shorter events, 0.6 us)
Async XLA Ops:
  0.0 242.7 %copy-start = (bf16[256,2048]{1,0:T(8,128)(2,1)S(1)}, bf16[256,2048]{1,0:T(8,128)(2,1)}, u32[]{:S(2)}) copy-start(bf16[256,2048]{1,0:T(8,128)(2,1)} %param.51) | copy-start | bytes 3145732
  8.6 1.0 copy-start.5
  9.6 86.1 %copy-start.2 = (bf16[64,2048]{1,0:T(8,128)(2,1)S(1)}, bf16[64,2048]{1,0:T(8,128)(2,1)}, u32[]{:S(2)}) copy-start(bf16[64,2048]{1,0:T(8,128)(2,1)} %param.29) | copy-start | bytes 786436
  95.7 2.6 %copy-start.1 = (f32[64,2048]{1,0:T(8,128)S(1)}, f32[64,2048]{1,0:T(8,128)}, u32[]{:S(2)}) copy-start(f32[64,2048]{1,0:T(8,128)} %shard_map.271) | copy-start | bytes 1572868
  95.7 2.6 %copy-start.6 = (f32[2048]{0:T(1024)S(1)}, f32[2048]{0:T(1024)}, u32[]{:S(2)}) copy-start(f32[2048]{0:T(1024)} %param.43) | copy-start | bytes 24580
  95.7 2.6 %copy-start.7 = (f32[2048]{0:T(1024)S(1)}, f32[2048]{0:T(1024)}, u32[]{:S(2)}) copy-start(f32[2048]{0:T(1024)} %param.42) | copy-start | bytes 24580
  95.8 2.8 %copy-start.10 = (s32[64,2]{0,1:T(2,128)S(1)}, s32[64,2]{0,1:T(2,128)}, u32[]{:S(2)}) copy-start(s32[64,2]{0,1:T(2,128)} %param.44) | copy-start | bytes 1540
  95.8 3.7 %copy-start.11 = (f32[64,2]{0,1:T(2,128)S(1)}, f32[64,2]{0,1:T(2,128)}, u32[]{:S(2)}) copy-start(f32[64,2]{0,1:T(2,128)} %param.45) | copy-start | bytes 1540
  101.7 140.7 %copy-start.3 = (bf16[2048,256]{1,0:T(8,128)(2,1)S(1)}, bf16[2048,256]{1,0:T(8,128)(2,1)}, u32[]{:S(2)}) copy-start(bf16[2048,256]{1,0:T(8,128)(2,1)} %param.49) | copy-start | bytes 3145732
  242.4 1.2 copy-start.4
  243.6 2.2 copy-start.8
  243.6 2.2 copy-start.9
